TPU v7x, 32 devices: a whole 2x2x4 slice. The times are simulated.
32 devices in a mesh: sp: 8 (over z, x), tp: 4 (over y, core).
Axes of the slice: x: 2, y: 2, z: 4, core: 2. Of those that a mesh axis runs over, the one named last changes fastest.
Arguments:
- layer_input: bfloat16 [1024, 2048], P('sp'), may hold values from -6 to 6
- out_cot: bfloat16 [1024, 2048], P('sp'), may hold values from -6 to 6
- routes: int32 [1024, 2], P('sp'), may hold values from 0 to 7, all different within a row; in each aligned block of 128 rows (0 to 127, 128 to 255, ...) at most 64 rows name the same one
- route_weights: float32 [1024, 2], P('sp'), may hold values from 0.2 to 1
- gate_weights: bfloat16 [8, 2048, 1024], P('sp', None, 'tp'), may hold values from -0.125 to 0.125
- up_weights: bfloat16 [8, 2048, 1024], P('sp', None, 'tp'), may hold values from -0.125 to 0.125
- down_weights: bfloat16 [8, 1024, 2048], P('sp', 'tp'), may hold values from -0.1875 to 0.1875
- out_proj: bfloat16 [2048, 2048], P(None, 'tp'), may hold values from -0.125 to 0.125
- queries: bfloat16 [1024, 2048], P('sp', 'tp'), may hold values from -6 to 6
- keys: bfloat16 [1024, 2048], P('sp', 'tp'), may hold values from -6 to 6
- values: bfloat16 [1024, 2048], P('sp', 'tp'), may hold values from -6 to 6
- mixer_out: bfloat16 [1024, 2048], P('sp', 'tp'), may hold values from -6 to 6
- entry_states: float32 [8, 32, 64, 64], P('sp', 'tp'), may hold values from -6 to 6
Outputs:
- grad_gate: bfloat16 [8, 2048, 1024], P('sp', None, 'tp')
- grad_up: bfloat16 [8, 2048, 1024], P('sp', None, 'tp')
- grad_down: bfloat16 [8, 1024, 2048], P('sp', 'tp')
- grad_proj: float32 [2048, 2048], P('sp', 'tp')
- grad_queries: bfloat16 [1024, 2048], P('sp', 'tp')
- grad_keys: bfloat16 [1024, 2048], P('sp', 'tp')
- grad_values: bfloat16 [1024, 2048], P('sp', 'tp')
Inputs may be any that keep to these rules, and one draw needn't show every extreme that they name: `routes`: in each aligned block of 128 rows no expert is named by more than 64 rows, a bound that some block reaches; the numbers of one row differ.
All inputs are finite; a program needn't handle non-finite values.
Results may differ from a plain program's by a relative error of at most 0.01.
Values may be sent and summed in bfloat16 or wider, within the bound.
A program may use at most 128 MiB of HBM per device.

v0:
```python
import jax
import jax.numpy as jnp
from jax import lax
from jax.sharding import PartitionSpec as P

DK = 64
SPAN = 128


def prefix(array, axis, combine, identity):
    devices, position = (lax.axis_size(axis), lax.axis_index(axis))
    everything = jax.tree.map(lambda part: lax.all_gather(part, axis), array)
    start = jax.tree.map(
        lambda part, zero: jnp.broadcast_to(jnp.asarray(zero, part.dtype), part.shape),
        array,
        identity,
    )

    def hop(k, before):
        at = devices - 1 - k
        reached = at > position
        new = combine(before, jax.tree.map(lambda part: part[at], everything))
        return jax.tree.map(lambda a, b: jnp.where(reached, a, b), new, before)

    return lax.fori_loop(0, devices, hop, start)


def decay_rates(head_ids, head_count, token_count):
    half_count = head_count // 2
    fraction = jnp.minimum(head_ids, half_count) / half_count
    base_rate = jnp.exp(
        (1.0 - fraction) * jnp.log(1.0 / 32.0) + fraction * jnp.log(1.0 / token_count)
    )
    return base_rate * (1.0 + jnp.maximum(head_ids - half_count, 0.0) / half_count)


def position_norm(positions, head_rates):
    return jnp.sqrt(
        jnp.expm1(-2.0 * head_rates)[None, :]
        / jnp.expm1(-2.0 * head_rates[None, :] * (positions[:, None] + 1.0))
    )


def expert_grads(exp_rows, exp_cot, activated, d_gate, d_up):
    row_dims = (((0,), (0,)), ((), ()))
    grad_gate = lax.dot_general(
        exp_rows, d_gate, row_dims, preferred_element_type=jnp.float32
    ).astype(jnp.bfloat16)
    grad_up = lax.dot_general(exp_rows, d_up, row_dims, preferred_element_type=jnp.float32).astype(
        jnp.bfloat16
    )
    grad_down = lax.dot_general(
        activated, exp_cot, row_dims, preferred_element_type=jnp.float32
    ).astype(jnp.bfloat16)
    return (grad_gate[None], grad_up[None], grad_down[None])


def later_first(earlier, later):
    return (earlier[0] * later[0], later[1] + later[0][:, None, None] * earlier[1])


def per_device(
    layer_input,
    out_cot,
    routes,
    route_weights,
    gate_weights,
    up_weights,
    down_weights,
    out_proj,
    queries,
    keys,
    values,
    mixer_out,
    entry_states,
):
    tok_rows, model_width = layer_input.shape
    experts = lax.axis_size("sp")
    narrow = lax.axis_size("tp")
    top_count = routes.shape[1]
    pair_count = tok_rows * top_count
    capacity = 2 * pair_count // experts
    flat_routes = routes.reshape(pair_count)
    onehot = (flat_routes[:, None] == jnp.arange(experts, dtype=jnp.int32)[None, :]).astype(
        jnp.int32
    )
    earlier = jnp.cumsum(onehot, axis=0) - onehot
    target = flat_routes * capacity + jnp.sum(earlier * onehot, axis=1)
    owner_tok = jnp.arange(pair_count, dtype=jnp.int32) // top_count
    slot_tok = jnp.full((experts * capacity,), tok_rows, jnp.int32).at[target].set(owner_tok)
    slot_weight = (
        jnp.zeros((experts * capacity,), jnp.float32)
        .at[target]
        .set(route_weights.reshape(pair_count))
    )
    blank_row = jnp.zeros((1, model_width), jnp.bfloat16)
    sent_rows = jnp.concatenate([layer_input, blank_row], 0)[slot_tok].reshape(
        experts, capacity, model_width
    )
    picked_cot = jnp.concatenate([out_cot, blank_row], 0)[slot_tok]
    sent_cot = (
        (slot_weight[:, None] * picked_cot.astype(jnp.float32))
        .astype(jnp.bfloat16)
        .reshape(experts, capacity, model_width)
    )
    share = capacity // narrow
    first_row = lax.axis_index("tp") * share
    part_rows = lax.dynamic_slice_in_dim(sent_rows, first_row, share, 1)
    part_cot = lax.dynamic_slice_in_dim(sent_cot, first_row, share, 1)
    got_rows, got_cot = (
        lax.all_to_all(part_rows, "sp", split_axis=0, concat_axis=0, tiled=True),
        lax.all_to_all(part_cot, "sp", split_axis=0, concat_axis=0, tiled=True),
    )
    got_rows, got_cot = (
        lax.all_gather(got_rows, "tp", axis=1, tiled=True),
        lax.all_gather(got_cot, "tp", axis=1, tiled=True),
    )
    exp_rows = got_rows.reshape(experts * capacity, model_width)
    exp_cot = got_cot.reshape(experts * capacity, model_width)
    gate_w = gate_weights[0]
    up_w = up_weights[0]
    down_w = down_weights[0]
    gate_pre = jnp.dot(exp_rows, gate_w, preferred_element_type=jnp.float32)
    up_pre = jnp.dot(exp_rows, up_w, preferred_element_type=jnp.float32)
    sigmoid_g = jax.nn.sigmoid(gate_pre)
    activated = (gate_pre * sigmoid_g * up_pre).astype(jnp.bfloat16)
    width_dims = (((1,), (1,)), ((), ()))
    d_act = lax.dot_general(exp_cot, down_w, width_dims, preferred_element_type=jnp.float32)
    d_gate = (d_act * up_pre * sigmoid_g * (1.0 + gate_pre * (1.0 - sigmoid_g))).astype(
        jnp.bfloat16
    )
    d_up = (d_act * gate_pre * sigmoid_g).astype(jnp.bfloat16)
    grads = expert_grads(exp_rows, exp_cot, activated, d_gate, d_up)
    partial_sum = lax.dot_general(d_gate, gate_w, width_dims, preferred_element_type=jnp.float32)
    partial_sum = partial_sum + lax.dot_general(
        d_up, up_w, width_dims, preferred_element_type=jnp.float32
    )
    summed = lax.psum_scatter(
        partial_sum.reshape(experts, capacity, model_width), "tp", scatter_dimension=2, tiled=True
    )
    returned = lax.all_to_all(
        summed.astype(jnp.bfloat16), "sp", split_axis=0, concat_axis=0, tiled=True
    )
    col_count = model_width // narrow
    first_col = lax.axis_index("tp") * col_count
    back_flat = returned.reshape(experts * capacity, col_count)
    pair_back = back_flat[target].reshape(tok_rows, top_count, col_count).astype(jnp.float32)
    own_cols = lax.dynamic_slice_in_dim(out_cot, first_col, col_count, 1).astype(jnp.float32)
    cot_cols = (own_cols + jnp.sum(pair_back, axis=1)).astype(jnp.bfloat16)
    mixer_cot = lax.all_gather(cot_cols, "tp", axis=1, tiled=True)
    grad_proj = lax.psum_scatter(
        lax.dot_general(
            mixer_cot, mixer_out, (((0,), (0,)), ((), ())), preferred_element_type=jnp.float32
        ),
        "sp",
        scatter_dimension=0,
        tiled=True,
    )
    head_count = queries.shape[1] // DK
    head_ids = (lax.axis_index("tp") * head_count + jnp.arange(head_count, dtype=jnp.int32)).astype(
        jnp.float32
    )
    head_rates = decay_rates(head_ids, head_count * narrow, tok_rows * experts)
    positions = (lax.axis_index("sp") * tok_rows + jnp.arange(tok_rows, dtype=jnp.int32)).astype(
        jnp.float32
    )
    head_cot = jnp.dot(mixer_cot, out_proj, preferred_element_type=jnp.float32).reshape(
        tok_rows, head_count, DK
    )
    head_cot = (head_cot * position_norm(positions, head_rates)[:, :, None]).astype(jnp.bfloat16)
    span_count = tok_rows // SPAN
    span_shape = (span_count, SPAN, head_count, DK)
    span_query = queries.reshape(span_shape)
    span_key = keys.reshape(span_shape)
    span_value = values.reshape(span_shape)
    span_cot = head_cot.reshape(span_shape)
    key_scale = DK ** (-0.5)
    offsets = jnp.arange(SPAN, dtype=jnp.float32)
    distance = offsets[:, None] - offsets[None, :]
    decay_mat = jnp.where(
        distance[None] >= 0,
        jnp.exp(-head_rates[:, None, None] * jnp.maximum(distance, 0.0)[None]),
        0.0,
    )
    fwd_weights = (
        jnp.einsum("cihd,cjhd->chij", span_query, span_key, preferred_element_type=jnp.float32)
        * key_scale
        * decay_mat[None]
    ).astype(jnp.bfloat16)
    back_weights = (
        jnp.einsum("cihd,cjhd->chij", span_cot, span_value, preferred_element_type=jnp.float32)
        * decay_mat[None]
    ).astype(jnp.bfloat16)
    tail_decay = jnp.exp(-head_rates[None, :] * (SPAN - 1.0 - offsets)[:, None])
    lead_decay = jnp.exp(-head_rates[None, :] * (offsets + 1.0)[:, None])
    span_decay = jnp.exp(-head_rates * SPAN)
    query_wide = span_query.astype(jnp.float32)
    key_wide = span_key.astype(jnp.float32)
    value_wide = span_value.astype(jnp.float32)
    cot_wide = span_cot.astype(jnp.float32)
    updates = key_scale * jnp.einsum(
        "cjhd,cjhe->chde",
        key_wide * tail_decay[None, :, :, None],
        value_wide,
        precision=lax.Precision.HIGHEST,
    )
    backs = jnp.einsum(
        "cihd,cihe->chde",
        query_wide * lead_decay[None, :, :, None],
        cot_wide,
        precision=lax.Precision.HIGHEST,
    )
    carried = entry_states[0]
    span_id = 0
    fwd_states = [carried]
    carried = span_decay[:, None, None] * carried + updates[span_id]
    reverse_state = jnp.zeros_like(carried)
    rev_local = [reverse_state] * span_count
    span_id = 0
    rev_local[span_id] = reverse_state
    reverse_state = span_decay[:, None, None] * reverse_state + backs[span_id]
    dev_decay = jnp.exp(-head_rates * tok_rows)
    identity = (jnp.ones_like(dev_decay), jnp.zeros_like(reverse_state))
    from_later = prefix((dev_decay, reverse_state), "sp", later_first, identity)[1]
    rev_states = jnp.stack(
        [
            rev_local[0]
            + jnp.exp(-head_rates * ((span_count - 1) * SPAN))[:, None, None] * from_later
        ]
    )
    fwd_stack = jnp.stack(fwd_states)
    grad_q = key_scale * jnp.einsum(
        "chij,cjhd->cihd", back_weights, span_key, preferred_element_type=jnp.float32
    )
    grad_q = grad_q + lead_decay[None, :, :, None] * jnp.einsum(
        "chde,cihe->cihd", fwd_stack, cot_wide, precision=lax.Precision.HIGHEST
    )
    grad_k = jnp.einsum(
        "chij,cihd->cjhd", back_weights, span_query, preferred_element_type=jnp.float32
    )
    grad_k = key_scale * (
        grad_k
        + tail_decay[None, :, :, None]
        * jnp.einsum("chde,cjhe->cjhd", rev_states, value_wide, precision=lax.Precision.HIGHEST)
    )
    grad_v = jnp.einsum(
        "chij,cihe->cjhe", fwd_weights, span_cot, preferred_element_type=jnp.float32
    )
    grad_v = grad_v + key_scale * tail_decay[None, :, :, None] * jnp.einsum(
        "chde,cjhd->cjhe", rev_states, key_wide, precision=lax.Precision.HIGHEST
    )
    flat_shape = (tok_rows, head_count * DK)
    return (
        grads[0],
        grads[1],
        grads[2],
        grad_proj,
        grad_q.reshape(flat_shape).astype(jnp.bfloat16),
        grad_k.reshape(flat_shape).astype(jnp.bfloat16),
        grad_v.reshape(flat_shape).astype(jnp.bfloat16),
    )


def solution(mesh):
    placed = (
        P("sp", None),
        P("sp", None),
        P("sp", None),
        P("sp", None),
        P("sp", None, "tp"),
        P("sp", None, "tp"),
        P("sp", "tp", None),
        P(None, "tp"),
        P("sp", "tp"),
        P("sp", "tp"),
        P("sp", "tp"),
        P("sp", "tp"),
        P("sp", "tp", None, None),
    )
    return jax.shard_map(
        per_device,
        mesh=mesh,
        in_specs=placed,
        out_specs=(
            P("sp", None, "tp"),
            P("sp", None, "tp"),
            P("sp", "tp", None),
            P("sp", "tp"),
            P("sp", "tp"),
            P("sp", "tp"),
            P("sp", "tp"),
        ),
        check_vma=False,
    )
```

profile of v0, /device:TPU:0, one launch (start us, length us, event | category | flops | bytes accessed | tf_op | source)
XLA Modules:
  0.0 315.5 jit_solution(11229628259408267841)
XLA Ops:
  10.3 1.4 scatter_custom_fusion
  12.9 3.3 %gather_fusion = bf16[512,2048]{1,0:T(8,128)(2,1)} fusion(bf16[129,2048]{1,0:T(8,128)(2,1)S(1)} %concatenate.6, s32[1024]{0:T(1024)S(1)} %pad_clamp_fusion.1), kind=kCustom, calls=%fused_computation | custom fusion | bytes 4196352 | tf_op jit(solution)/shard_map/gather | solution.py:97
  17.3 21.7 %all_to_all.15 = bf16[8,16,2048]{2,1,0:T(8,128)(2,1)} all-to-all(bf16[8,16,2048]{2,1,0:T(8,128)(2,1)S(1)} %constant_dynamic-slice_fusion.1), channel_id=1, replica_groups=mesh['sp'=8,'tp'=4] {'sp'}, dimensions={0} | all-to-all | bytes 1048576 | tf_op jit(solution)/shard_map/all_to_all | solution.py:111
  39.4 1.4 scatter_custom_fusion.1
  40.9 3.3 %gather_fusion.1 = bf16[512,2048]{1,0:T(8,128)(2,1)} fusion(bf16[129,2048]{1,0:T(8,128)(2,1)S(1)} %concatenate.7, s32[1024]{0:T(1024)S(1)} %pad_clamp_fusion.1), kind=kCustom, calls=%fused_computation.1 | custom fusion | bytes 4196352 | tf_op jit(solution)/shard_map/gather | solution.py:100
  45.5 17.6 %all_to_all.16 = bf16[8,16,2048]{2,1,0:T(8,128)(2,1)} all-to-all(bf16[8,16,2048]{2,1,0:T(8,128)(2,1)S(1)} %fusion.18), channel_id=1, replica_groups=mesh['sp'=8,'tp'=4] {'sp'}, dimensions={0} | all-to-all | bytes 1048576 | tf_op jit(solution)/shard_map/all_to_all | solution.py:112
  63.2 3.5 %fusion.21 = f32[512,256]{1,0:T(8,128)} fusion(bf16[512,2048]{1,0:T(8,128)(2,1)} %bitcast.165, bf16[1,2048,256]{2,1,0:T(8,128)(2,1)} %param.19), kind=kOutput, calls=%fused_computation.42 | convolution fusion | flops 536870912 | bytes 3670016 | tf_op jit(solution)/shard_map/dot_general | solution.py:123
  66.8 1.5 fusion.24
  68.3 16.7 %all-gather.8.cloned.1.call-done = bf16[8,64,2048]{2,1,0:T(8,128)(2,1)} async-done(((bf16[8,16,2048]{2,1,0:T(8,128)(2,1)}), bf16[8,64,2048]{2,1,0:T(8,128)(2,1)}) %all-gather.8.cloned.1.call-update) | async-done | bytes 2097168 | tf_op jit(solution)/shard_map/all_gather | solution.py:116
  85.0 3.0 multiply_convert_fusion.1
  88.8 2.8 convolution_add_fusion
  91.6 44.6 %reduce-scatter.3.cloned.1.call-done = f32[8,64,512]{2,1,0:T(8,128)} async-done(((f32[8,64,2048]{2,1,0:T(8,128)}), f32[8,64,512]{2,1,0:T(8,128)}) %reduce-scatter.3.cloned.1.call-update) | async-done | bytes 1048592 | tf_op jit(solution)/shard_map/reduce_scatter | solution.py:138
  136.2 2.1 convert_element_type.144
  138.3 5.5 %all-to-all-start.2 = ((bf16[8,64,512]{2,1,0:T(8,128)(2,1)}), bf16[8,64,512]{2,1,0:T(8,128)(2,1)S(1)}, u32[]{:S(2)}, u32[]{:S(2)}) async-start(bf16[8,64,512]{2,1,0:T(8,128)(2,1)} %convert_element_type.144), calls=%async_computation.3 | async-start | bytes 1048576 | tf_op jit(solution)/shard_map/all_to_all | solution.py:141
  144.2 13.9 %all-to-all-done.2 = bf16[8,64,512]{2,1,0:T(8,128)(2,1)S(1)} async-done(((bf16[8,64,512]{2,1,0:T(8,128)(2,1)}), bf16[8,64,512]{2,1,0:T(8,128)(2,1)S(1)}, u32[]{:S(2)}, u32[]{:S(2)}) %all-to-all-start.2) | async-done | bytes 524320 | tf_op jit(solution)/shard_map/all_to_all | solution.py:141
  161.2 6.7 %all_gather.19 = bf16[128,2048]{1,0:T(8,128)(2,1)S(1)} all-gather(bf16[128,512]{1,0:T(8,128)(2,1)S(1)} %add_convert_fusion), channel_id=1, replica_groups=mesh['sp'=8,'tp'=4] {'tp'}, dimensions={1}, use_global_device_ids=true | all-gather | bytes 655360 | tf_op jit(solution)/shard_map/all_gather | solution.py:150
  169.9 2.7 fusion.56
  173.8 19.2 %all-gather.1 = f32[8,1,8]{2,1,0:T(1,128)S(1)} all-gather(f32[1,1,8]{2,1,0:T(1,128)S(1)} %exponential_bitcast_fusion), channel_id=1, replica_groups=mesh['sp'=8,'tp'=4] {'sp'}, dimensions={0}, use_global_device_ids=true | all-gather | bytes 288 | tf_op jit(solution)/shard_map/all_gather | solution.py:12
  193.1 3.5 %fusion.1 = bf16[1,2048,256]{2,1,0:T(8,128)(2,1)} fusion(bf16[512,2048]{1,0:T(8,128)(2,1)} %bitcast.166, bf16[512,256]{1,0:T(8,128)(2,1)S(1)} %copy-done.9), kind=kOutput, calls=%fused_computation.12 | convolution fusion | flops 537395200 | bytes 3407872 | tf_op jit(solution)/shard_map/dot_general | solution.py:46
  196.6 1.8 fusion.2
  198.7 1.8 fusion.3
  202.1 15.9 %all-gather.10.cloned.1.call-done = f32[64,64,64]{2,1,0:T(8,128)} async-done(((f32[8,64,64]{2,1,0:T(8,128)}), f32[64,64,64]{2,1,0:T(8,128)}) %all-gather.10.cloned.1.call-update) | async-done | bytes 1048592 | tf_op jit(solution)/shard_map/all_gather | solution.py:12
  218.0 8.8 %while.16 = (s32[]{:T(128)}, f32[8,64,64]{2,1,0:T(8,128)S(1)}, s32[]{:T(128)}, f32[8,8,64,64]{3,2,1,0:T(8,128)}, f32[8,8]{1,0:T(8,128)S(1)}, /*index=5*/s32[]{:T(128)}, s32[]{:T(128)}, s32[]{:T(128)}, s32[]{:T(128)}) while((s32[]{:T(128)}, f32[8,64,64]{2,1,0:T(8,128)S(1)}, s32[]{:T(128)}, f32[8,8,64,64]{3,2,1,0:T(8,128)}, ...), condition=%wide.region_9.10_spmd.clone, body=%wide.region_8.9_spmd.clone.sunk | while | flops 131080 | bytes 393487 | solution.py:25
  229.8 79.2 %reduce-scatter.5.cloned.1.call-done = f32[256,512]{1,0:T(8,128)} async-done(((f32[2048,512]{1,0:T(8,128)}), f32[256,512]{1,0:T(8,128)}) %reduce-scatter.5.cloned.1.call-update) | async-done | bytes 524304 | tf_op jit(solution)/shard_map/reduce_scatter | solution.py:151
  (118 shorter events, 28.1 us)
Async XLA Ops:
  7.2 160.7 %copy-start = (bf16[2048,512]{1,0:T(8,128)(2,1)S(1)}, bf16[2048,512]{1,0:T(8,128)(2,1)}, u32[]{:S(2)}) copy-start(bf16[2048,512]{1,0:T(8,128)(2,1)} %param.22) | copy-start | bytes 6291460
  7.2 56.0 %all-gather.6.cloned.1.call-start = ((), (), s32[]{:S(2)}) async-start(), calls=%async_computation.5 | async-start | bytes 2621440 | tf_op jit(solution)/shard_map/all_gather | solution.py:115
  16.2 22.9 %copy-start.14 = (f32[128,2]{0,1:T(2,128)S(1)}, f32[128,2]{0,1:T(2,128)}, u32[]{:S(2)}) copy-start(f32[128,2]{0,1:T(2,128)} %param.18) | copy-start | bytes 3076
  16.2 24.7 %copy-start.4 = (bf16[128,2048]{1,0:T(8,128)(2,1)S(1)}, bf16[128,2048]{1,0:T(8,128)(2,1)}, u32[]{:S(2)}) copy-start(bf16[128,2048]{1,0:T(8,128)(2,1)} %param.16) | copy-start | bytes 1572868
  39.1 45.9 %all-gather.8.cloned.1.call-start = ((), (), s32[]{:S(2)}) async-start(), calls=%async_computation.6 | async-start | bytes 2621440 | tf_op jit(solution)/shard_map/all_gather | solution.py:116
  63.1 3.6 %copy-start.2 = (bf16[1,2048,256]{2,1,0:T(8,128)(2,1)S(1)}, bf16[1,2048,256]{2,1,0:T(8,128)(2,1)}, u32[]{:S(2)}) copy-start(bf16[1,2048,256]{2,1,0:T(8,128)(2,1)} %param.20) | copy-start | bytes 3145732
  63.2 73.0 %reduce-scatter.3.cloned.1.call-start = ((), (), s32[]{:S(2)}) async-start(), calls=%async_computation.7 | async-start | bytes 5242880 | tf_op jit(solution)/shard_map/reduce_scatter | solution.py:138
  63.2 3.5 %copy-start.15 = (bf16[8,64,2048]{2,1,0:T(8,128)(2,1)S(1)}, bf16[8,64,2048]{2,1,0:T(8,128)(2,1)}, u32[]{:S(2)}) copy-start(bf16[8,64,2048]{2,1,0:T(8,128)(2,1)} %all-gather.6.cloned.1.call-done) | copy-start | bytes 6291460
  85.0 3.1 copy-start.3
  88.0 0.8 copy-start.8
  91.6 52.2 %copy-start.11 = (bf16[128,512]{1,0:T(8,128)(2,1)S(1)}, bf16[128,512]{1,0:T(8,128)(2,1)}, u32[]{:S(2)}) copy-start(bf16[128,512]{1,0:T(8,128)(2,1)} %param.23) | copy-start | bytes 393220
  138.3 19.8 %all-to-all-start.2 = ((bf16[8,64,512]{2,1,0:T(8,128)(2,1)}), bf16[8,64,512]{2,1,0:T(8,128)(2,1)S(1)}, u32[]{:S(2)}, u32[]{:S(2)}) async-start(bf16[8,64,512]{2,1,0:T(8,128)(2,1)} %convert_element_type.144), calls=%async_computation.3 | async-start | bytes 1048576 | tf_op jit(solution)/shard_map/all_to_all | solution.py:141
  143.8 74.2 %all-gather.10.cloned.1.call-start = ((), (), s32[]{:S(2)}) async-start(), calls=%async_computation.9 | async-start | bytes 2359296 | tf_op jit(solution)/shard_map/all_gather | solution.py:12
  167.8 2.1 copy-start.10
  169.9 139.1 %reduce-scatter.5.cloned.1.call-start = ((), (), s32[]{:S(2)}) async-start(), calls=%async_computation.8 | async-start | bytes 4718592 | tf_op jit(solution)/shard_map/reduce_scatter | solution.py:151
  172.6 0.9 copy-start.12
  172.6 1.0 copy-start.13
  172.6 20.5 %copy-start.9 = (bf16[512,256]{1,0:T(8,128)(2,1)S(1)}, bf16[512,256]{1,0:T(8,128)(2,1)}, u32[]{:S(2)}) copy-start(bf16[512,256]{1,0:T(8,128)(2,1)} %copy-done.8) | copy-start | bytes 786436
  193.1 3.5 %copy-start.16 = (bf16[8,64,2048]{2,1,0:T(8,128)(2,1)S(1)}, bf16[8,64,2048]{2,1,0:T(8,128)(2,1)}, u32[]{:S(2)}) copy-start(bf16[8,64,2048]{2,1,0:T(8,128)(2,1)} %all-gather.6.cloned.1.call-done) | copy-start | bytes 6291460
  196.6 1.8 copy-start.1
  196.6 1.8 copy-start.5
  196.6 2.2 copy-start.6
  198.7 2.3 copy-start.7
Sparse Core Ops, SparseCore 0:
  39.2 21.5 all-gather.5
  63.3 21.6 all-gather.7
  91.7 44.4 reduce-scatter.2
  170.0 47.9 all-gather.9
  222.0 86.8 reduce-scatter.4
where the time goes:
time: 316 us; the launch traced here: 315 us
  waiting for transfers between devices  170 us (54%)
  blocking collectives  65.2 us (21%)
  matrix products  25.4 us (8%)
  local copies, waits for them, and re-layouts  19.2 us (6%)
  other arithmetic  15.2 us (5%)
  between operations  14.2 us (4%)
  starting transfers between devices  5.69 us (2%)
    reduce_scatter x1, waiting for transfers between devices, per_device(): lax.psum_scatter(lax.dot_general(mixer_cot, mixer_out, (((0,), (0,)), (()...  79.2 us
    reduce_scatter x1, waiting for transfers between devices, per_device(): lax.psum_scatter(partial_sum.reshape(experts, capacity, model_width), 'tp...  44.6 us
    all_to_all x1, blocking collectives, per_device(): lax.all_to_all(part_rows, 'sp', split_axis=0, concat_axis=0, tiled=True)  21.7 us
    all_gather x1, blocking collectives, prefix(): everything = jax.tree.map(lambda part: lax.all_gather(part, axis), array)  19.2 us
    all_to_all x1, blocking collectives, per_device(): lax.all_to_all(part_cot, 'sp', split_axis=0, concat_axis=0, tiled=True)  17.6 us
    all_gather x1, waiting for transfers between devices, per_device(): lax.all_gather(got_cot, 'tp', axis=1, tiled=True)  16.7 us
    all_gather x1, waiting for transfers between devices, prefix(): everything = jax.tree.map(lambda part: lax.all_gather(part, axis), array)  15.9 us
    all_to_all x1, waiting for transfers between devices, per_device(): lax.all_to_all(summed.astype(jnp.bfloat16), 'sp', split_axis=0, concat_ax...  13.9 us
  transfers between devices with their start and end apart: 6, of which 5 were waited for; matrix products, arithmetic and copies ran while one was open for 11% of the time, Pallas kernels for 0%

commit v1 on v0

--- a/solution.py
+++ b/solution.py
@@ -1,28 +1,283 @@
+import functools
+
 import jax
 import jax.numpy as jnp
 from jax import lax
+from jax.experimental import pallas as pl
+from jax.experimental.pallas import tpu as pltpu
 from jax.sharding import PartitionSpec as P
 
 DK = 64
 SPAN = 128
-
-
-def prefix(array, axis, combine, identity):
-    devices, position = (lax.axis_size(axis), lax.axis_index(axis))
-    everything = jax.tree.map(lambda part: lax.all_gather(part, axis), array)
-    start = jax.tree.map(
-        lambda part, zero: jnp.broadcast_to(jnp.asarray(zero, part.dtype), part.shape),
-        array,
-        identity,
-    )
-
-    def hop(k, before):
-        at = devices - 1 - k
-        reached = at > position
-        new = combine(before, jax.tree.map(lambda part: part[at], everything))
-        return jax.tree.map(lambda a, b: jnp.where(reached, a, b), new, before)
-
-    return lax.fori_loop(0, devices, hop, start)
+MESH = pl.DeviceIdType.MESH
+VMEM = pl.BlockSpec(memory_space=pltpu.VMEM)
+
+
+def seat(experts):
+    me, tp = lax.axis_index("sp"), lax.axis_index("tp")
+    core, row = tp % 2, tp // 2
+    return me, tp, core, row, tp + 1 - 2 * core, (tp + 2) % 4
+
+
+def greet(experts, me, tp_peers):
+    barrier = pltpu.get_barrier_semaphore()
+    for k in range(1, experts):
+        pl.semaphore_signal(
+            barrier, inc=1, device_id={"sp": (me + k) % experts}, device_id_type=MESH
+        )
+    for peer in tp_peers:
+        pl.semaphore_signal(barrier, inc=1, device_id={"tp": peer}, device_id_type=MESH)
+    pl.semaphore_wait(barrier, experts - 1 + len(tp_peers))
+
+
+def send(src, dst, send_sem, recv_sem, target):
+    copy = pltpu.make_async_remote_copy(
+        src_ref=src,
+        dst_ref=dst,
+        send_sem=send_sem,
+        recv_sem=recv_sem,
+        device_id=target,
+        device_id_type=MESH,
+    )
+    copy.start()
+    return copy
+
+
+def dispatch_kernel(
+    experts, rows, cot, out_rows, out_cot, own, s_sp, r_sp, s_y, r_y, s_c, r_c
+):
+    me, tp, core, row, mate, across = seat(experts)
+    greet(experts, me, (mate, across))
+    arrays = ((rows, out_rows), (cot, out_cot))
+    far = {}
+    for k in range(1, experts):
+        peer = (me + k) % experts
+        for a, (src, dst) in enumerate(arrays):
+            far[a, k] = send(
+                src.at[peer], dst.at[me, tp], s_sp.at[a, k], r_sp.at[a, k], {"sp": peer}
+            )
+    local = []
+    for a, (src, dst) in enumerate(arrays):
+        copy = pltpu.make_async_copy(src.at[me], dst.at[me, tp], own.at[a])
+        copy.start()
+        local.append(copy)
+    for copy in local:
+        copy.wait()
+    side, near, relayed = {}, {}, {}
+
+    def relay(k):
+        origin = (me - k + experts) % experts
+        for a, (src, dst) in enumerate(arrays):
+            side[a, k].wait_recv()
+            held = dst.at[origin, across]
+            relayed[a, k] = send(held, held, s_c.at[a, 1, k], r_c.at[a, 1, k], {"tp": mate})
+
+    for k in range(experts):
+        origin = (me - k + experts) % experts
+        for a, (src, dst) in enumerate(arrays):
+            if k > 0:
+                far[a, k].wait_recv()
+            held = dst.at[origin, tp]
+            side[a, k] = send(held, held, s_y.at[a, k], r_y.at[a, k], {"tp": across})
+            near[a, k] = send(held, held, s_c.at[a, 0, k], r_c.at[a, 0, k], {"tp": mate})
+        if k > 1:
+            relay(k - 2)
+    relay(experts - 2)
+    relay(experts - 1)
+    for copy in list(near.values()) + list(relayed.values()):
+        copy.wait_recv()
+    for group in (far, side, near, relayed):
+        for copy in group.values():
+            copy.wait_send()
+
+
+def dispatch(rows, cot, narrow):
+    experts, share, width = rows.shape
+    full = jax.ShapeDtypeStruct((experts, narrow, share, width), rows.dtype)
+    sem = pltpu.SemaphoreType.DMA
+    return pl.pallas_call(
+        functools.partial(dispatch_kernel, experts),
+        out_shape=(full, full),
+        in_specs=[VMEM, VMEM],
+        out_specs=(VMEM, VMEM),
+        scratch_shapes=[
+            sem((2,)),
+            sem((2, experts)),
+            sem((2, experts)),
+            sem((2, experts)),
+            sem((2, experts)),
+            sem((2, 2, experts)),
+            sem((2, 2, experts)),
+        ],
+        compiler_params=pltpu.CompilerParams(collective_id=0, has_side_effects=True),
+    )(rows, cot)
+
+
+def combine_kernel(
+    experts,
+    part,
+    picks,
+    own_cot,
+    mixer,
+    near_buf,
+    side_out,
+    side_in,
+    far_out,
+    back,
+    s_c,
+    r_c,
+    s_y,
+    r_y,
+    s_f,
+    r_f,
+    s_g,
+    r_g,
+):
+    me, tp, core, row, mate, across = seat(experts)
+    cols = part.shape[2] // 4
+
+    def quarter(index):
+        return pl.ds(pl.multiple_of(index * cols, cols), cols)
+
+    greet(experts, me, (mate, across))
+    order = list(range(1, experts)) + [0]
+    near, side, far = {}, {}, {}
+    mate_core = 1 - core
+    for k in order:
+        dest = (me + k) % experts
+        for half in range(2):
+            near[k, half] = send(
+                part.at[dest, :, quarter(half * 2 + mate_core)],
+                near_buf.at[k, half],
+                s_c.at[k, half],
+                r_c.at[k, half],
+                {"tp": mate},
+            )
+    for k in order:
+        dest = (me + k) % experts
+        near[k, 0].wait_recv()
+        near[k, 1].wait_recv()
+        side_out[k] = (
+            part[dest, :, quarter(across)].astype(jnp.float32)
+            + near_buf[k, 1 - row].astype(jnp.float32)
+        ).astype(jnp.bfloat16)
+        side[k] = send(side_out.at[k], side_in.at[k], s_y.at[k], r_y.at[k], {"tp": across})
+    for k in order:
+        dest = (me + k) % experts
+        side[k].wait_recv()
+        done = (
+            part[dest, :, quarter(tp)].astype(jnp.float32)
+            + near_buf[k, row].astype(jnp.float32)
+            + side_in[k].astype(jnp.float32)
+        ).astype(jnp.bfloat16)
+        if k == 0:
+            back[me] = done
+        else:
+            far_out[k] = done
+            far[k] = send(far_out.at[k], back.at[me], s_f.at[k], r_f.at[k], {"sp": dest})
+    for k in range(1, experts):
+        far[k].wait_recv()
+    slots = back[...].reshape(experts * part.shape[1], cols)
+    total = own_cot[:, quarter(tp)].astype(jnp.float32) + jnp.dot(
+        picks[...], slots, preferred_element_type=jnp.float32
+    )
+    mixer[:, quarter(tp)] = total.astype(jnp.bfloat16)
+    mine = mixer.at[:, quarter(tp)]
+    other = mixer.at[:, quarter(across)]
+    last = [
+        send(mine, mine, s_g.at[0], r_g.at[0], {"tp": across}),
+        send(mine, mine, s_g.at[1], r_g.at[1], {"tp": mate}),
+    ]
+    last[0].wait_recv()
+    last.append(send(other, other, s_g.at[2], r_g.at[2], {"tp": mate}))
+    last[1].wait_recv()
+    last[2].wait_recv()
+    for group in (near.values(), side.values(), far.values(), last):
+        for copy in group:
+            copy.wait_send()
+
+
+def combine(part, picks, own_cot):
+    experts, capacity, width = part.shape
+    tok_rows = own_cot.shape[0]
+    cols = width // 4
+    sem = pltpu.SemaphoreType.DMA
+    block = pltpu.VMEM((experts, capacity, cols), jnp.bfloat16)
+    return pl.pallas_call(
+        functools.partial(combine_kernel, experts),
+        out_shape=jax.ShapeDtypeStruct((tok_rows, width), jnp.bfloat16),
+        in_specs=[VMEM, VMEM, VMEM],
+        out_specs=VMEM,
+        scratch_shapes=[
+            pltpu.VMEM((experts, 2, capacity, cols), jnp.bfloat16),
+            block,
+            block,
+            block,
+            block,
+            sem((experts, 2)),
+            sem((experts, 2)),
+            sem((experts,)),
+            sem((experts,)),
+            sem((experts,)),
+            sem((experts,)),
+            sem((3,)),
+            sem((3,)),
+        ],
+        compiler_params=pltpu.CompilerParams(collective_id=1, has_side_effects=True),
+    )(part, picks, own_cot)
+
+
+def spread_kernel(experts, mixer, state, all_mixer, all_state, own, s_m, r_m, s_s, r_s):
+    me = lax.axis_index("sp")
+    cols = mixer.shape[1] // experts
+    greet(experts, me, ())
+
+    def block(index):
+        return mixer.at[:, pl.ds(pl.multiple_of(index * cols, cols), cols)]
+
+    copies = []
+    for k in range(1, experts):
+        peer = (me + k) % experts
+        copies.append(send(state, all_state.at[me], s_s.at[k], r_s.at[k], {"sp": peer}))
+    for k in range(1, experts):
+        peer = (me + k) % experts
+        copies.append(
+            send(block(peer), all_mixer.at[me], s_m.at[k], r_m.at[k], {"sp": peer})
+        )
+    local = [
+        pltpu.make_async_copy(state, all_state.at[me], own.at[0]),
+        pltpu.make_async_copy(block(me), all_mixer.at[me], own.at[1]),
+    ]
+    for copy in local:
+        copy.start()
+    for copy in local:
+        copy.wait()
+    for copy in copies:
+        copy.wait_recv()
+    for copy in copies:
+        copy.wait_send()
+
+
+def spread(mixer, state, experts):
+    sem = pltpu.SemaphoreType.DMA
+    tok_rows, width = mixer.shape
+    return pl.pallas_call(
+        functools.partial(spread_kernel, experts),
+        out_shape=(
+            jax.ShapeDtypeStruct((experts, tok_rows, width // experts), mixer.dtype),
+            jax.ShapeDtypeStruct((experts,) + state.shape, state.dtype),
+        ),
+        in_specs=[VMEM, VMEM],
+        out_specs=(VMEM, VMEM),
+        scratch_shapes=[
+            sem((2,)),
+            sem((experts,)),
+            sem((experts,)),
+            sem((experts,)),
+            sem((experts,)),
+        ],
+        compiler_params=pltpu.CompilerParams(collective_id=2, has_side_effects=True),
+    )(mixer, state)
 
 
 def decay_rates(head_ids, head_count, token_count):
@@ -53,10 +308,6 @@
         activated, exp_cot, row_dims, preferred_element_type=jnp.float32
     ).astype(jnp.bfloat16)
     return (grad_gate[None], grad_up[None], grad_down[None])
-
-
-def later_first(earlier, later):
-    return (earlier[0] * later[0], later[1] + later[0][:, None, None] * earlier[1])
 
 
 def per_device(
@@ -86,35 +337,59 @@
     )
     earlier = jnp.cumsum(onehot, axis=0) - onehot
     target = flat_routes * capacity + jnp.sum(earlier * onehot, axis=1)
-    owner_tok = jnp.arange(pair_count, dtype=jnp.int32) // top_count
-    slot_tok = jnp.full((experts * capacity,), tok_rows, jnp.int32).at[target].set(owner_tok)
-    slot_weight = (
-        jnp.zeros((experts * capacity,), jnp.float32)
-        .at[target]
-        .set(route_weights.reshape(pair_count))
-    )
-    blank_row = jnp.zeros((1, model_width), jnp.bfloat16)
-    sent_rows = jnp.concatenate([layer_input, blank_row], 0)[slot_tok].reshape(
-        experts, capacity, model_width
-    )
-    picked_cot = jnp.concatenate([out_cot, blank_row], 0)[slot_tok]
-    sent_cot = (
-        (slot_weight[:, None] * picked_cot.astype(jnp.float32))
-        .astype(jnp.bfloat16)
-        .reshape(experts, capacity, model_width)
-    )
     share = capacity // narrow
     first_row = lax.axis_index("tp") * share
-    part_rows = lax.dynamic_slice_in_dim(sent_rows, first_row, share, 1)
-    part_cot = lax.dynamic_slice_in_dim(sent_cot, first_row, share, 1)
-    got_rows, got_cot = (
-        lax.all_to_all(part_rows, "sp", split_axis=0, concat_axis=0, tiled=True),
-        lax.all_to_all(part_cot, "sp", split_axis=0, concat_axis=0, tiled=True),
-    )
-    got_rows, got_cot = (
-        lax.all_gather(got_rows, "tp", axis=1, tiled=True),
-        lax.all_gather(got_cot, "tp", axis=1, tiled=True),
-    )
+    fused = narrow == 4 and share % 16 == 0 and model_width % (experts * 128) == 0
+    if fused:
+        pair_slot = target.reshape(tok_rows, top_count)
+        part_slot = (
+            jnp.arange(experts, dtype=jnp.int32)[:, None] * capacity
+            + first_row
+            + jnp.arange(share, dtype=jnp.int32)[None, :]
+        ).reshape(experts * share)
+        hits = part_slot[:, None, None] == pair_slot[None]
+        part_weight = jnp.sum(jnp.where(hits, route_weights[None], 0.0), axis=(1, 2))
+        chosen = jnp.any(hits, axis=2).astype(jnp.bfloat16)
+        part_rows = jnp.dot(chosen, layer_input, preferred_element_type=jnp.float32)
+        part_cot = jnp.dot(chosen, out_cot, preferred_element_type=jnp.float32)
+        part_shape = (experts, share, model_width)
+        got_rows, got_cot = dispatch(
+            part_rows.astype(jnp.bfloat16).reshape(part_shape),
+            (part_weight[:, None] * part_cot).astype(jnp.bfloat16).reshape(part_shape),
+            narrow,
+        )
+        all_slots = jnp.arange(experts * capacity, dtype=jnp.int32)
+        picks = jnp.any(pair_slot[:, :, None] == all_slots[None, None], axis=1).astype(
+            jnp.bfloat16
+        )
+    else:
+        owner_tok = jnp.arange(pair_count, dtype=jnp.int32) // top_count
+        slot_tok = jnp.full((experts * capacity,), tok_rows, jnp.int32).at[target].set(owner_tok)
+        slot_weight = (
+            jnp.zeros((experts * capacity,), jnp.float32)
+            .at[target]
+            .set(route_weights.reshape(pair_count))
+        )
+        blank_row = jnp.zeros((1, model_width), jnp.bfloat16)
+        sent_rows = jnp.concatenate([layer_input, blank_row], 0)[slot_tok].reshape(
+            experts, capacity, model_width
+        )
+        picked_cot = jnp.concatenate([out_cot, blank_row], 0)[slot_tok]
+        sent_cot = (
+            (slot_weight[:, None] * picked_cot.astype(jnp.float32))
+            .astype(jnp.bfloat16)
+            .reshape(experts, capacity, model_width)
+        )
+        part_rows = lax.dynamic_slice_in_dim(sent_rows, first_row, share, 1)
+        part_cot = lax.dynamic_slice_in_dim(sent_cot, first_row, share, 1)
+        got_rows, got_cot = (
+            lax.all_to_all(part_rows, "sp", split_axis=0, concat_axis=0, tiled=True),
+            lax.all_to_all(part_cot, "sp", split_axis=0, concat_axis=0, tiled=True),
+        )
+        got_rows, got_cot = (
+            lax.all_gather(got_rows, "tp", axis=1, tiled=True),
+            lax.all_gather(got_cot, "tp", axis=1, tiled=True),
+        )
     exp_rows = got_rows.reshape(experts * capacity, model_width)
     exp_cot = got_cot.reshape(experts * capacity, model_width)
     gate_w = gate_weights[0]
@@ -135,27 +410,26 @@
     partial_sum = partial_sum + lax.dot_general(
         d_up, up_w, width_dims, preferred_element_type=jnp.float32
     )
-    summed = lax.psum_scatter(
-        partial_sum.reshape(experts, capacity, model_width), "tp", scatter_dimension=2, tiled=True
-    )
-    returned = lax.all_to_all(
-        summed.astype(jnp.bfloat16), "sp", split_axis=0, concat_axis=0, tiled=True
-    )
-    col_count = model_width // narrow
-    first_col = lax.axis_index("tp") * col_count
-    back_flat = returned.reshape(experts * capacity, col_count)
-    pair_back = back_flat[target].reshape(tok_rows, top_count, col_count).astype(jnp.float32)
-    own_cols = lax.dynamic_slice_in_dim(out_cot, first_col, col_count, 1).astype(jnp.float32)
-    cot_cols = (own_cols + jnp.sum(pair_back, axis=1)).astype(jnp.bfloat16)
-    mixer_cot = lax.all_gather(cot_cols, "tp", axis=1, tiled=True)
-    grad_proj = lax.psum_scatter(
-        lax.dot_general(
-            mixer_cot, mixer_out, (((0,), (0,)), ((), ())), preferred_element_type=jnp.float32
-        ),
-        "sp",
-        scatter_dimension=0,
-        tiled=True,
-    )
+    if fused:
+        mixer_cot = combine(
+            partial_sum.astype(jnp.bfloat16).reshape(experts, capacity, model_width),
+            picks,
+            out_cot,
+        )
+    else:
+        summed = lax.psum_scatter(
+            partial_sum.reshape(experts, capacity, model_width), "tp", scatter_dimension=2, tiled=True
+        )
+        returned = lax.all_to_all(
+            summed.astype(jnp.bfloat16), "sp", split_axis=0, concat_axis=0, tiled=True
+        )
+        col_count = model_width // narrow
+        first_col = lax.axis_index("tp") * col_count
+        back_flat = returned.reshape(experts * capacity, col_count)
+        pair_back = back_flat[target].reshape(tok_rows, top_count, col_count).astype(jnp.float32)
+        own_cols = lax.dynamic_slice_in_dim(out_cot, first_col, col_count, 1).astype(jnp.float32)
+        cot_cols = (own_cols + jnp.sum(pair_back, axis=1)).astype(jnp.bfloat16)
+        mixer_cot = lax.all_gather(cot_cols, "tp", axis=1, tiled=True)
     head_count = queries.shape[1] // DK
     head_ids = (lax.axis_index("tp") * head_count + jnp.arange(head_count, dtype=jnp.int32)).astype(
         jnp.float32
@@ -193,42 +467,56 @@
     ).astype(jnp.bfloat16)
     tail_decay = jnp.exp(-head_rates[None, :] * (SPAN - 1.0 - offsets)[:, None])
     lead_decay = jnp.exp(-head_rates[None, :] * (offsets + 1.0)[:, None])
-    span_decay = jnp.exp(-head_rates * SPAN)
     query_wide = span_query.astype(jnp.float32)
     key_wide = span_key.astype(jnp.float32)
     value_wide = span_value.astype(jnp.float32)
     cot_wide = span_cot.astype(jnp.float32)
-    updates = key_scale * jnp.einsum(
-        "cjhd,cjhe->chde",
-        key_wide * tail_decay[None, :, :, None],
-        value_wide,
-        precision=lax.Precision.HIGHEST,
-    )
     backs = jnp.einsum(
         "cihd,cihe->chde",
         query_wide * lead_decay[None, :, :, None],
         cot_wide,
         precision=lax.Precision.HIGHEST,
     )
-    carried = entry_states[0]
-    span_id = 0
-    fwd_states = [carried]
-    carried = span_decay[:, None, None] * carried + updates[span_id]
-    reverse_state = jnp.zeros_like(carried)
-    rev_local = [reverse_state] * span_count
-    span_id = 0
-    rev_local[span_id] = reverse_state
-    reverse_state = span_decay[:, None, None] * reverse_state + backs[span_id]
-    dev_decay = jnp.exp(-head_rates * tok_rows)
-    identity = (jnp.ones_like(dev_decay), jnp.zeros_like(reverse_state))
-    from_later = prefix((dev_decay, reverse_state), "sp", later_first, identity)[1]
-    rev_states = jnp.stack(
-        [
-            rev_local[0]
-            + jnp.exp(-head_rates * ((span_count - 1) * SPAN))[:, None, None] * from_later
-        ]
-    )
-    fwd_stack = jnp.stack(fwd_states)
+    own_back = backs[0]
+    if fused:
+        packed = own_back.astype(jnp.bfloat16).reshape(head_count * DK // 2, 2 * DK)
+        all_mixer, all_backs = spread(mixer_cot, packed, experts)
+        all_backs = all_backs.reshape((experts,) + own_back.shape).astype(jnp.float32)
+        all_out = jnp.concatenate(
+            [mixer_out]
+            + [
+                lax.ppermute(mixer_out, "sp", [(i, (i + k) % experts) for i in range(experts)])
+                for k in range(1, experts)
+            ],
+            axis=0,
+        )
+        device = lax.axis_index("sp")
+        sources = (device - jnp.arange(experts)) % experts
+        all_mixer = all_mixer[sources]
+        grad_proj = lax.dot_general(
+            all_mixer.reshape(experts * tok_rows, model_width // experts),
+            all_out,
+            (((0,), (0,)), ((), ())),
+            preferred_element_type=jnp.float32,
+        )
+    else:
+        all_backs = lax.all_gather(own_back, "sp")
+        grad_proj = lax.psum_scatter(
+            lax.dot_general(
+                mixer_cot, mixer_out, (((0,), (0,)), ((), ())), preferred_element_type=jnp.float32
+            ),
+            "sp",
+            scatter_dimension=0,
+            tiled=True,
+        )
+    ahead = jnp.arange(experts, dtype=jnp.int32) - lax.axis_index("sp") - 1
+    reach = jnp.where(
+        ahead[:, None] >= 0,
+        jnp.exp(-head_rates[None, :] * (jnp.maximum(ahead, 0) * tok_rows)[:, None]),
+        0.0,
+    )
+    rev_states = jnp.sum(reach[:, :, None, None] * all_backs, axis=0)[None]
+    fwd_stack = entry_states
     grad_q = key_scale * jnp.einsum(
         "chij,cjhd->cihd", back_weights, span_key, preferred_element_type=jnp.float32
     )

time: 316 us -> 183 us (0.58)
  waiting for transfers between devices: 170 us -> 0.02 us
  Pallas kernels: 0 us -> 101 us
  blocking collectives: 65.2 us -> 0 us
  between operations: 14.2 us -> 1 us
  starting transfers between devices: 5.69 us -> 17.9 us
  other arithmetic: 15.2 us -> 6.66 us
  matrix products: 25.4 us -> 32.8 us
  local copies, waits for them, and re-layouts: 19.2 us -> 22.4 us
    reduce_scatter x2 -> x0, waiting for transfers between devices: 124 us -> none  [the longest x1 79.2 us: per_device(): lax.psum_scatter(lax.dot_general(mixer_cot, mixer_out, (((0,), (0,)), (()...]
    pallas_call x0 -> x3, Pallas kernels: none -> 101 us  [the longest x1 40.5 us: dispatch(): pl.pallas_call(functools.partial(dispatch_kernel, experts), out_shape=(fu...]
    all_to_all x2 -> x0, blocking collectives: 39.3 us -> none  [the longest x1 21.7 us: per_device(): lax.all_to_all(part_rows, 'sp', split_axis=0, concat_axis=0, tiled=True)]
    all_gather x3 -> x0, waiting for transfers between devices: 32.6 us -> none  [the longest x1 16.7 us: per_device(): lax.all_gather(got_cot, 'tp', axis=1, tiled=True)]
    all_gather x2 -> x0, blocking collectives: 25.9 us -> none  [the longest x1 19.2 us: prefix(): everything = jax.tree.map(lambda part: lax.all_gather(part, axis), array)]
    ppermute x0 -> x7, starting transfers between devices: none -> 17.9 us  [per_device(): lax.ppermute(mixer_out, 'sp', [(i, (i + k) % experts) for i in range(expe...]
    all_to_all x1 -> x0, waiting for transfers between devices: 13.9 us -> none  [per_device(): lax.all_to_all(summed.astype(jnp.bfloat16), 'sp', split_axis=0, concat_ax...]
    unnamed x42 -> x44, local copies, waits for them, and re-layouts: 4.91 us -> 15.1 us
  transfers between devices with their start and end apart: 6 -> 7, of which waited for: 5 -> 0; matrix products, arithmetic and copies ran while one was open for 11% -> 32% of each run, Pallas kernels for 0% -> 56%
where the time goes in v1:
time: 183 us; the launch traced here: 182 us
  Pallas kernels  101 us (55%)
  matrix products  32.8 us (18%)
  local copies, waits for them, and re-layouts  22.4 us (12%)
  starting transfers between devices  17.9 us (10%)
  other arithmetic  6.66 us (4%)
    pallas_call x1, Pallas kernels, dispatch(): pl.pallas_call(functools.partial(dispatch_kernel, experts), out_shape=(fu...  40.5 us
    pallas_call x1, Pallas kernels, combine(): pl.pallas_call(functools.partial(combine_kernel, experts), out_shape=jax....  32.9 us
    pallas_call x1, Pallas kernels, spread(): pl.pallas_call(functools.partial(spread_kernel, experts), out_shape=(jax....  27.7 us
    ppermute x7, starting transfers between devices, per_device(): lax.ppermute(mixer_out, 'sp', [(i, (i + k) % experts) for i in range(expe...  17.9 us
    unnamed x44, local copies, waits for them, and re-layouts  15.1 us
  transfers between devices with their start and end apart: 7, of which 0 were waited for; matrix products, arithmetic and copies ran while one was open for 32% of the time, Pallas kernels for 56%

profile of v1, /device:TPU:0, one launch (start us, length us, event | category | flops | bytes accessed | tf_op | source)
XLA Modules:
  0.0 181.8 jit_solution(17775565522943379325)
XLA Ops:
  0.7 3.0 %collective-permute-start = (bf16[128,512]{1,0:T(8,128)(2,1)}, bf16[128,512]{1,0:T(8,128)(2,1)}, u32[]{:S(2)}, u32[]{:S(2)}) collective-permute-start(bf16[128,512]{1,0:T(8,128)(2,1)} %param.24), channel_id=1, source_target_pairs={{0,4},{4,8},{8,12},{12,16},{16,20},{20,24},{24,28},{28,0},{1,5},{5... | collective-permute-start | bytes 393224 | tf_op jit(solution)/shard_map/ppermute | solution.py:488
  3.7 1.6 collective-permute-start.1
  5.3 2.6 %collective-permute-start.2 = (bf16[128,512]{1,0:T(8,128)(2,1)}, bf16[128,512]{1,0:T(8,128)(2,1)}, u32[]{:S(2)}, u32[]{:S(2)}) collective-permute-start(bf16[128,512]{1,0:T(8,128)(2,1)} %param.24), channel_id=1, source_target_pairs={{0,12},{4,16},{8,20},{12,24},{16,28},{20,0},{24,4},{28,8},{1,13},{... | collective-permute-start | bytes 393224 | tf_op jit(solution)/shard_map/ppermute | solution.py:488
  9.1 2.6 %collective-permute-start.4 = (bf16[128,512]{1,0:T(8,128)(2,1)}, bf16[128,512]{1,0:T(8,128)(2,1)}, u32[]{:S(2)}, u32[]{:S(2)}) collective-permute-start(bf16[128,512]{1,0:T(8,128)(2,1)} %param.24), channel_id=1, source_target_pairs={{0,20},{4,24},{8,28},{12,0},{16,4},{20,8},{24,12},{28,16},{1,21},{... | collective-permute-start | bytes 393224 | tf_op jit(solution)/shard_map/ppermute | solution.py:488
  15.7 2.1 %convolution_convert_fusion.3 = bf16[128,2048]{1,0:T(8,128)(2,1)} fusion(pred[128,128]{1,0:T(8,128)(4,1)S(1)} %compare_reduce_fusion, bf16[128,2048]{1,0:T(8,128)(2,1)} %param.13), kind=kOutput, calls=%fused_computation.10 | convolution fusion | flops 67371008 | bytes 1064960 | tf_op jit(solution)/shard_map/dot_general | solution.py:353
  17.9 2.1 %fusion.3 = bf16[128,2048]{1,0:T(8,128)(2,1)} fusion(pred[128,128]{1,0:T(8,128)(4,1)S(1)} %compare_reduce_fusion, bf16[128,2048]{1,0:T(8,128)(2,1)} %own_cot.1, f32[128]{0:T(128)S(1)} %fusion.37), kind=kOutput, calls=%fused_computation.9 | convolution fusion | flops 67633152 | bytes 1065472 | tf_op jit(solution)/shard_map/dot_general | solution.py:354
  20.0 40.5 %shard_map.180 = (bf16[8,4,16,2048]{3,2,1,0:T(8,128)(2,1)}, bf16[8,4,16,2048]{3,2,1,0:T(8,128)(2,1)}) custom-call(bf16[8,16,2048]{2,1,0:T(8,128)(2,1)} %bitcast.137, bf16[8,16,2048]{2,1,0:T(8,128)(2,1)} %bitcast.138), custom_call_target="tpu_custom_call" | custom-call | tf_op jit(solution)/shard_map/pallas_call | solution.py:98
  60.5 2.5 %fusion.20 = f32[512,256]{1,0:T(8,128)S(1)} fusion(bf16[512,2048]{1,0:T(8,128)(2,1)} %bitcast.152, bf16[1,2048,256]{2,1,0:T(8,128)(2,1)S(1)} %copy-done.3), kind=kOutput, calls=%fused_computation.36 | convolution fusion | flops 536870912 | bytes 3670016 | tf_op jit(solution)/shard_map/dot_general | solution.py:398
  64.6 1.8 fusion.2
  67.2 1.7 fusion
  68.9 2.7 %fusion.18 = f32[512,2048]{1,0:T(8,128)} fusion(bf16[512,256]{1,0:T(8,128)(2,1)S(1)} %get-tuple-element.44, bf16[1,2048,256]{2,1,0:T(8,128)(2,1)S(1)} %copy-done.3), kind=kOutput, calls=%fused_computation.34 | convolution fusion | flops 536870912 | bytes 5505024 | tf_op jit(solution)/shard_map/dot_general | solution.py:409
  73.8 3.5 %fusion.1 = bf16[1,2048,256]{2,1,0:T(8,128)(2,1)} fusion(bf16[512,2048]{1,0:T(8,128)(2,1)} %bitcast.153, bf16[512,256]{1,0:T(8,128)(2,1)S(1)} %get-tuple-element.43), kind=kOutput, calls=%fused_computation.6 | convolution fusion | flops 537395200 | bytes 3407872 | tf_op jit(solution)/shard_map/dot_general | solution.py:304
  77.3 2.1 %add_convert_fusion = bf16[512,2048]{1,0:T(8,128)(2,1)} fusion(f32[512,2048]{1,0:T(8,128)S(1)} %copy-done.1, bf16[512,256]{1,0:T(8,128)(2,1)S(1)} %get-tuple-element.43, bf16[1,2048,256]{2,1,0:T(8,128)(2,1)S(1)} %copy-done.5), kind=kOutput, calls=%fused_computation.1 | convolution fusion | flops 538968064 | bytes 7602176 | tf_op jit(solution)/shard_map/dot_general | solution.py:410
  80.1 32.9 %shard_map.181.mixer = bf16[128,2048]{1,0:T(8,128)(2,1)} custom-call(bf16[8,64,2048]{2,1,0:T(8,128)(2,1)} %bitcast.134, bf16[128,512]{1,0:T(8,128)(2,1)} %convert_element_type.135.picks, bf16[128,2048]{1,0:T(8,128)(2,1)} %own_cot.1), custom_call_target="tpu_custom_call" | custom-call | tf_op jit(solution)/shard_map/pallas_call | solution.py:206
  113.1 2.0 %fusion.52 = f32[128,512]{0,1:T(8,128)S(1)} fusion(bf16[128,2048]{1,0:T(8,128)(2,1)} %shard_map.181.mixer, bf16[2048,512]{1,0:T(8,128)(2,1)S(1)} %copy-done), kind=kOutput, calls=%fused_computation.111 | convolution fusion | flops 268435456 | bytes 2883584 | tf_op jit(solution)/shard_map/dot_general | solution.py:441
  116.4 27.7 %shard_map.182 = (bf16[8,128,256]{2,1,0:T(8,128)(2,1)}, bf16[8,256,128]{2,1,0:T(8,128)(2,1)}) custom-call(bf16[128,2048]{1,0:T(8,128)(2,1)} %shard_map.181.mixer, bf16[256,128]{1,0:T(8,128)(2,1)} %convert_element_type.141.state), custom_call_target="tpu_custom_call" | custom-call | tf_op jit(solution)/shard_map/pallas_call | solution.py:264
  146.6 2.0 %mul.366 = f32[8,256,128]{2,1,0:T(8,128)S(1)} reshape(f32[8,8,64,64]{3,2,1,0:T(8,128)} %mul.365) | data formatting | bytes 2097152 | tf_op jit(solution)/shard_map/mul | solution.py:518
  148.6 1.8 multiply_reduce_fusion
  156.1 2.1 %fusion.17 = bf16[1,128,8,64]{1,3,2,0:T(8,128)(2,1)} fusion(f32[1,128,8,64]{1,3,2,0:T(8,128)} %fusion.14, bf16[128,8,64]{0,2,1:T(8,128)(2,1)S(1)} %multiply_convert_fusion.4, bf16[128,8,64]{0,2,1:T(8,128)(2,1)S(1)} %bitcast.145, bf16[128,8,64]{0,2,1:T(8,128)(2,1)S(1)} %bitcast.142, f32[128,128]{1,0:T(8,128)} %fusion.39, f32[8]{0:T(128)S(1)} %get-tuple-element.49, ...), kind=kOutput, calls=%fused_computation.33 | convolution fusion | flops 34340864 | bytes 868384 | tf_op jit(solution)/shard_map/chij,cihe->cjhe/dot_general | solution.py:534
  161.0 1.7 copy.71
  163.3 5.1 %collective-permute-start.5 = (bf16[128,512]{1,0:T(8,128)(2,1)S(1)}, bf16[128,512]{1,0:T(8,128)(2,1)S(1)}, u32[]{:S(2)}, u32[]{:S(2)}) collective-permute-start(bf16[128,512]{1,0:T(8,128)(2,1)S(1)} %copy-done.12), channel_id=1, source_target_pairs={{0,24},{4,28},{8,0},{12,4},{16,8},{20,12},{24,16},{28,20},{1,25},{... | collective-permute-start | bytes 393224 | tf_op jit(solution)/shard_map/ppermute | solution.py:488
  170.0 1.8 collective-permute-start.6
  171.8 1.6 constant_dynamic-update-slice_fusion.5
  179.4 2.5 %fusion.53 = f32[256,512]{1,0:T(8,128)} fusion(bf16[1024,256]{1,0:T(8,128)(2,1)S(1)} %bitcast.139, bf16[1024,512]{1,0:T(8,128)(2,1)} %constant_dynamic-update-slice_fusion), kind=kOutput, calls=%fused_computation.112 | convolution fusion | flops 268435456 | bytes 2097152 | tf_op jit(solution)/shard_map/dot_general | solution.py:496
  (96 shorter events, 31.0 us)
Async XLA Ops:
  0.6 112.4 %copy-start = (bf16[2048,512]{1,0:T(8,128)(2,1)S(1)}, bf16[2048,512]{1,0:T(8,128)(2,1)}, u32[]{:S(2)}) copy-start(bf16[2048,512]{1,0:T(8,128)(2,1)} %param.20) | copy-start | bytes 6291460
  0.6 59.8 %copy-start.3 = (bf16[1,2048,256]{2,1,0:T(8,128)(2,1)S(1)}, bf16[1,2048,256]{2,1,0:T(8,128)(2,1)}, u32[]{:S(2)}) copy-start(bf16[1,2048,256]{2,1,0:T(8,128)(2,1)} %param.17) | copy-start | bytes 3145732
  0.7 162.6 %collective-permute-start = (bf16[128,512]{1,0:T(8,128)(2,1)}, bf16[128,512]{1,0:T(8,128)(2,1)}, u32[]{:S(2)}, u32[]{:S(2)}) collective-permute-start(bf16[128,512]{1,0:T(8,128)(2,1)} %param.24), channel_id=1, source_target_pairs={{0,4},{4,8},{8,12},{12,16},{16,20},{20,24},{24,28},{28,0},{1,5},{5... | collective-permute-start | bytes 393224 | tf_op jit(solution)/shard_map/ppermute | solution.py:488
  3.7 166.3 %collective-permute-start.1 = (bf16[128,512]{1,0:T(8,128)(2,1)}, bf16[128,512]{1,0:T(8,128)(2,1)}, u32[]{:S(2)}, u32[]{:S(2)}) collective-permute-start(bf16[128,512]{1,0:T(8,128)(2,1)} %param.24), channel_id=1, source_target_pairs={{0,8},{4,12},{8,16},{12,20},{16,24},{20,28},{24,0},{28,4},{1,9},{5... | collective-permute-start | bytes 393224 | tf_op jit(solution)/shard_map/ppermute | solution.py:488
  5.3 168.1 %collective-permute-start.2 = (bf16[128,512]{1,0:T(8,128)(2,1)}, bf16[128,512]{1,0:T(8,128)(2,1)}, u32[]{:S(2)}, u32[]{:S(2)}) collective-permute-start(bf16[128,512]{1,0:T(8,128)(2,1)} %param.24), channel_id=1, source_target_pairs={{0,12},{4,16},{8,20},{12,24},{16,28},{20,0},{24,4},{28,8},{1,13},{... | collective-permute-start | bytes 393224 | tf_op jit(solution)/shard_map/ppermute | solution.py:488
  7.8 167.1 %collective-permute-start.3 = (bf16[128,512]{1,0:T(8,128)(2,1)}, bf16[128,512]{1,0:T(8,128)(2,1)}, u32[]{:S(2)}, u32[]{:S(2)}) collective-permute-start(bf16[128,512]{1,0:T(8,128)(2,1)} %param.24), channel_id=1, source_target_pairs={{0,16},{4,20},{8,24},{12,28},{16,0},{20,4},{24,8},{28,12},{1,17},{... | collective-permute-start | bytes 393224 | tf_op jit(solution)/shard_map/ppermute | solution.py:488
  9.1 167.4 %collective-permute-start.4 = (bf16[128,512]{1,0:T(8,128)(2,1)}, bf16[128,512]{1,0:T(8,128)(2,1)}, u32[]{:S(2)}, u32[]{:S(2)}) collective-permute-start(bf16[128,512]{1,0:T(8,128)(2,1)} %param.24), channel_id=1, source_target_pairs={{0,20},{4,24},{8,28},{12,0},{16,4},{20,8},{24,12},{28,16},{1,21},{... | collective-permute-start | bytes 393224 | tf_op jit(solution)/shard_map/ppermute | solution.py:488
  60.5 2.5 %copy-start.4 = (bf16[1,2048,256]{2,1,0:T(8,128)(2,1)S(1)}, bf16[1,2048,256]{2,1,0:T(8,128)(2,1)}, u32[]{:S(2)}) copy-start(bf16[1,2048,256]{2,1,0:T(8,128)(2,1)} %param.18) | copy-start | bytes 3145732
  60.5 2.5 %copy-start.13 = (bf16[8,4,16,2048]{3,2,1,0:T(8,128)(2,1)S(1)}, bf16[8,4,16,2048]{3,2,1,0:T(8,128)(2,1)}, u32[]{:S(2)}) copy-start(bf16[8,4,16,2048]{3,2,1,0:T(8,128)(2,1)} %get-tuple-element.11) | copy-start | bytes 6291460
  63.0 1.6 copy-start.2
  64.6 1.8 copy-start.14
  68.9 2.9 %copy-start.11 = (bf16[128,512]{1,0:T(8,128)(2,1)S(1)}, bf16[128,512]{1,0:T(8,128)(2,1)}, u32[]{:S(2)}) copy-start(bf16[128,512]{1,0:T(8,128)(2,1)} %param.24) | copy-start | bytes 393220
  73.8 3.5 %copy-start.1 = (f32[512,2048]{1,0:T(8,128)S(1)}, f32[512,2048]{1,0:T(8,128)}, u32[]{:S(2)}) copy-start(f32[512,2048]{1,0:T(8,128)} %fusion.18) | copy-start | bytes 12582916
  73.8 3.5 %copy-start.5 = (bf16[1,2048,256]{2,1,0:T(8,128)(2,1)S(1)}, bf16[1,2048,256]{2,1,0:T(8,128)(2,1)}, u32[]{:S(2)}) copy-start(bf16[1,2048,256]{2,1,0:T(8,128)(2,1)} %param.18) | copy-start | bytes 3145732
  77.3 2.8 %copy-start.8 = (bf16[128,512]{1,0:T(8,128)(2,1)S(1)}, bf16[128,512]{1,0:T(8,128)(2,1)}, u32[]{:S(2)}) copy-start(bf16[128,512]{1,0:T(8,128)(2,1)} %param.21) | copy-start | bytes 393220
  113.0 31.1 %copy-start.9 = (bf16[128,512]{1,0:T(8,128)(2,1)S(1)}, bf16[128,512]{1,0:T(8,128)(2,1)}, u32[]{:S(2)}) copy-start(bf16[128,512]{1,0:T(8,128)(2,1)} %param.23) | copy-start | bytes 393220
  113.1 31.8 %copy-start.10 = (bf16[128,512]{1,0:T(8,128)(2,1)S(1)}, bf16[128,512]{1,0:T(8,128)(2,1)}, u32[]{:S(2)}) copy-start(bf16[128,512]{1,0:T(8,128)(2,1)} %param.22) | copy-start | bytes 393220
  154.1 8.6 %copy-start.6 = (bf16[8,128,256]{2,1,0:T(8,128)(2,1)S(1)}, bf16[8,128,256]{2,1,0:T(8,128)(2,1)}, u32[]{:S(2)}) copy-start(bf16[8,128,256]{2,1,0:T(8,128)(2,1)} %get-tuple-element.13) | copy-start | bytes 1572868
  156.1 4.1 %copy-start.7 = (bf16[1,128,8,64]{1,3,2,0:T(8,128)(2,1)S(1)}, bf16[1,128,8,64]{1,3,2,0:T(8,128)(2,1)}, u32[]{:S(2)}) copy-start(bf16[1,128,8,64]{1,3,2,0:T(8,128)(2,1)} %fusion.16) | copy-start | bytes 393220
  156.1 7.2 %copy-start.12 = (bf16[128,512]{1,0:T(8,128)(2,1)S(1)}, bf16[128,512]{1,0:T(8,128)(2,1)}, u32[]{:S(2)}) copy-start(bf16[128,512]{1,0:T(8,128)(2,1)} %param.24) | copy-start | bytes 393220
  163.3 14.7 %collective-permute-start.5 = (bf16[128,512]{1,0:T(8,128)(2,1)S(1)}, bf16[128,512]{1,0:T(8,128)(2,1)S(1)}, u32[]{:S(2)}, u32[]{:S(2)}) collective-permute-start(bf16[128,512]{1,0:T(8,128)(2,1)S(1)} %copy-done.12), channel_id=1, source_target_pairs={{0,24},{4,28},{8,0},{12,4},{16,8},{20,12},{24,16},{28,20},{1,25},{... | collective-permute-start | bytes 393224 | tf_op jit(solution)/shard_map/ppermute | solution.py:488
  170.0 8.7 %collective-permute-start.6 = (bf16[128,512]{1,0:T(8,128)(2,1)S(1)}, bf16[128,512]{1,0:T(8,128)(2,1)S(1)}, u32[]{:S(2)}, u32[]{:S(2)}) collective-permute-start(bf16[128,512]{1,0:T(8,128)(2,1)S(1)} %copy-done.12), channel_id=1, source_target_pairs={{0,28},{4,0},{8,4},{12,8},{16,12},{20,16},{24,20},{28,24},{1,29},{... | collective-permute-start | bytes 393224 | tf_op jit(solution)/shard_map/ppermute | solution.py:488

commit v2 on v1

--- a/solution.py
+++ b/solution.py
@@ -41,6 +41,34 @@
     )
     copy.start()
     return copy
+
+
+def share_rows(experts, me, src, whole, own, s_r, r_r):
+    mate = me + 1 - 2 * (me % 2)
+    hops = []
+    for k in range(1, experts // 2):
+        peer = (me + 2 * k) % experts
+        hops.append(send(src, whole.at[me], s_r.at[0, k], r_r.at[0, k], {"sp": peer}))
+    relays = [send(src, whole.at[me], s_r.at[1, 0], r_r.at[1, 0], {"sp": mate})]
+    local = pltpu.make_async_copy(src, whole.at[me], own)
+    local.start()
+
+    def relay():
+        for k in range(1, experts // 2):
+            hops[k - 1].wait_recv()
+            held = whole.at[(me - 2 * k + experts) % experts]
+            relays.append(send(held, held, s_r.at[1, k], r_r.at[1, k], {"sp": mate}))
+
+    def arrive():
+        local.wait()
+        for copy in relays:
+            copy.wait_recv()
+
+    def drain():
+        for copy in hops + relays:
+            copy.wait_send()
+
+    return relay, arrive, drain
 
 
 def dispatch_kernel(
@@ -118,7 +146,9 @@
     part,
     picks,
     own_cot,
+    out_rows,
     mixer,
+    all_out,
     near_buf,
     side_out,
     side_in,
@@ -132,6 +162,9 @@
     r_f,
     s_g,
     r_g,
+    own,
+    s_r,
+    r_r,
 ):
     me, tp, core, row, mate, across = seat(experts)
     cols = part.shape[2] // 4
@@ -141,6 +174,7 @@
 
     greet(experts, me, (mate, across))
     order = list(range(1, experts)) + [0]
+    relay, arrive, drain = share_rows(experts, me, out_rows, all_out, own.at[0], s_r, r_r)
     near, side, far = {}, {}, {}
     mate_core = 1 - core
     for k in order:
@@ -175,6 +209,7 @@
         else:
             far_out[k] = done
             far[k] = send(far_out.at[k], back.at[me], s_f.at[k], r_f.at[k], {"sp": dest})
+    relay()
     for k in range(1, experts):
         far[k].wait_recv()
     slots = back[...].reshape(experts * part.shape[1], cols)
@@ -192,12 +227,14 @@
     last.append(send(other, other, s_g.at[2], r_g.at[2], {"tp": mate}))
     last[1].wait_recv()
     last[2].wait_recv()
+    arrive()
+    drain()
     for group in (near.values(), side.values(), far.values(), last):
         for copy in group:
             copy.wait_send()
 
 
-def combine(part, picks, own_cot):
+def combine(part, picks, own_cot, out_rows):
     experts, capacity, width = part.shape
     tok_rows = own_cot.shape[0]
     cols = width // 4
@@ -205,9 +242,12 @@
     block = pltpu.VMEM((experts, capacity, cols), jnp.bfloat16)
     return pl.pallas_call(
         functools.partial(combine_kernel, experts),
-        out_shape=jax.ShapeDtypeStruct((tok_rows, width), jnp.bfloat16),
-        in_specs=[VMEM, VMEM, VMEM],
-        out_specs=VMEM,
+        out_shape=(
+            jax.ShapeDtypeStruct((tok_rows, width), jnp.bfloat16),
+            jax.ShapeDtypeStruct((experts,) + out_rows.shape, out_rows.dtype),
+        ),
+        in_specs=[VMEM, VMEM, VMEM, VMEM],
+        out_specs=(VMEM, VMEM),
         scratch_shapes=[
             pltpu.VMEM((experts, 2, capacity, cols), jnp.bfloat16),
             block,
@@ -222,12 +262,17 @@
             sem((experts,)),
             sem((3,)),
             sem((3,)),
+            sem((1,)),
+            sem((2, experts // 2)),
+            sem((2, experts // 2)),
         ],
         compiler_params=pltpu.CompilerParams(collective_id=1, has_side_effects=True),
-    )(part, picks, own_cot)
-
-
-def spread_kernel(experts, mixer, state, all_mixer, all_state, own, s_m, r_m, s_s, r_s):
+    )(part, picks, own_cot, out_rows)
+
+
+def spread_kernel(
+    experts, mixer, state, reach, all_mixer, later, all_state, own, s_m, r_m, s_r, r_r
+):
     me = lax.axis_index("sp")
     cols = mixer.shape[1] // experts
     greet(experts, me, ())
@@ -235,49 +280,51 @@
     def block(index):
         return mixer.at[:, pl.ds(pl.multiple_of(index * cols, cols), cols)]
 
+    relay, arrive, drain = share_rows(experts, me, state, all_state, own.at[0], s_r, r_r)
     copies = []
-    for k in range(1, experts):
-        peer = (me + k) % experts
-        copies.append(send(state, all_state.at[me], s_s.at[k], r_s.at[k], {"sp": peer}))
     for k in range(1, experts):
         peer = (me + k) % experts
         copies.append(
             send(block(peer), all_mixer.at[me], s_m.at[k], r_m.at[k], {"sp": peer})
         )
-    local = [
-        pltpu.make_async_copy(state, all_state.at[me], own.at[0]),
-        pltpu.make_async_copy(block(me), all_mixer.at[me], own.at[1]),
-    ]
-    for copy in local:
-        copy.start()
-    for copy in local:
-        copy.wait()
+    local = pltpu.make_async_copy(block(me), all_mixer.at[me], own.at[1])
+    local.start()
+    relay()
+    local.wait()
+    arrive()
+    total = jnp.zeros(later.shape, jnp.float32)
+    for j in range(experts):
+        total = total + reach[:, j : j + 1] * all_state[j].astype(jnp.float32)
+    later[...] = total
     for copy in copies:
         copy.wait_recv()
     for copy in copies:
         copy.wait_send()
-
-
-def spread(mixer, state, experts):
+    drain()
+
+
+def spread(mixer, state, reach):
     sem = pltpu.SemaphoreType.DMA
     tok_rows, width = mixer.shape
+    experts = reach.shape[1]
     return pl.pallas_call(
         functools.partial(spread_kernel, experts),
         out_shape=(
             jax.ShapeDtypeStruct((experts, tok_rows, width // experts), mixer.dtype),
-            jax.ShapeDtypeStruct((experts,) + state.shape, state.dtype),
+            jax.ShapeDtypeStruct(state.shape, jnp.float32),
         ),
-        in_specs=[VMEM, VMEM],
+        in_specs=[VMEM, VMEM, VMEM],
         out_specs=(VMEM, VMEM),
         scratch_shapes=[
+            pltpu.VMEM((experts,) + state.shape, state.dtype),
             sem((2,)),
             sem((experts,)),
             sem((experts,)),
-            sem((experts,)),
-            sem((experts,)),
+            sem((2, experts // 2)),
+            sem((2, experts // 2)),
         ],
         compiler_params=pltpu.CompilerParams(collective_id=2, has_side_effects=True),
-    )(mixer, state)
+    )(mixer, state, reach)
 
 
 def decay_rates(head_ids, head_count, token_count):
@@ -339,7 +386,7 @@
     target = flat_routes * capacity + jnp.sum(earlier * onehot, axis=1)
     share = capacity // narrow
     first_row = lax.axis_index("tp") * share
-    fused = narrow == 4 and share % 16 == 0 and model_width % (experts * 128) == 0
+    fused = narrow == 4 and experts % 2 == 0 and share % 16 == 0 and model_width % (experts * 128) == 0
     if fused:
         pair_slot = target.reshape(tok_rows, top_count)
         part_slot = (
@@ -411,10 +458,11 @@
         d_up, up_w, width_dims, preferred_element_type=jnp.float32
     )
     if fused:
-        mixer_cot = combine(
+        mixer_cot, all_out = combine(
             partial_sum.astype(jnp.bfloat16).reshape(experts, capacity, model_width),
             picks,
             out_cot,
+            mixer_out,
         )
     else:
         summed = lax.psum_scatter(
@@ -478,29 +526,27 @@
         precision=lax.Precision.HIGHEST,
     )
     own_back = backs[0]
+    ahead = jnp.arange(experts, dtype=jnp.int32) - lax.axis_index("sp") - 1
+    reach = jnp.where(
+        ahead[:, None] >= 0,
+        jnp.exp(-head_rates[None, :] * (jnp.maximum(ahead, 0) * tok_rows)[:, None]),
+        0.0,
+    )
     if fused:
         packed = own_back.astype(jnp.bfloat16).reshape(head_count * DK // 2, 2 * DK)
-        all_mixer, all_backs = spread(mixer_cot, packed, experts)
-        all_backs = all_backs.reshape((experts,) + own_back.shape).astype(jnp.float32)
-        all_out = jnp.concatenate(
-            [mixer_out]
-            + [
-                lax.ppermute(mixer_out, "sp", [(i, (i + k) % experts) for i in range(experts)])
-                for k in range(1, experts)
-            ],
-            axis=0,
-        )
-        device = lax.axis_index("sp")
-        sources = (device - jnp.arange(experts)) % experts
-        all_mixer = all_mixer[sources]
+        all_mixer, later = spread(
+            mixer_cot, packed, jnp.repeat(reach.T, DK // 2, axis=0)
+        )
+        rev_states = later.reshape((1,) + own_back.shape)
         grad_proj = lax.dot_general(
             all_mixer.reshape(experts * tok_rows, model_width // experts),
-            all_out,
+            all_out.reshape(experts * tok_rows, mixer_out.shape[1]),
             (((0,), (0,)), ((), ())),
             preferred_element_type=jnp.float32,
         )
     else:
         all_backs = lax.all_gather(own_back, "sp")
+        rev_states = jnp.sum(reach[:, :, None, None] * all_backs, axis=0)[None]
         grad_proj = lax.psum_scatter(
             lax.dot_general(
                 mixer_cot, mixer_out, (((0,), (0,)), ((), ())), preferred_element_type=jnp.float32
@@ -509,13 +555,6 @@
             scatter_dimension=0,
             tiled=True,
         )
-    ahead = jnp.arange(experts, dtype=jnp.int32) - lax.axis_index("sp") - 1
-    reach = jnp.where(
-        ahead[:, None] >= 0,
-        jnp.exp(-head_rates[None, :] * (jnp.maximum(ahead, 0) * tok_rows)[:, None]),
-        0.0,
-    )
-    rev_states = jnp.sum(reach[:, :, None, None] * all_backs, axis=0)[None]
     fwd_stack = entry_states
     grad_q = key_scale * jnp.einsum(
         "chij,cjhd->cihd", back_weights, span_key, preferred_element_type=jnp.float32

time: 183 us -> 141 us (0.77)
  starting transfers between devices: 17.9 us -> 0 us
  local copies, waits for them, and re-layouts: 22.4 us -> 8.04 us
  matrix products: 32.8 us -> 23.9 us
  other arithmetic: 6.66 us -> 4.56 us
  Pallas kernels: 101 us -> 103 us
    ppermute x7 -> x0, starting transfers between devices: 17.9 us -> none  [per_device(): lax.ppermute(mixer_out, 'sp', [(i, (i + k) % experts) for i in range(expe...]
    unnamed x44 -> x29, local copies, waits for them, and re-layouts: 15.1 us -> 5.75 us
    pallas_call x1, Pallas kernels: 32.9 us -> 37.7 us  [combine(): pl.pallas_call(functools.partial(combine_kernel, experts), out_shape=(jax...]
    pallas_call x1, Pallas kernels: 27.7 us -> 24 us  [spread(): pl.pallas_call(functools.partial(spread_kernel, experts), out_shape=(jax....]
    mul x2 -> x0, local copies, waits for them, and re-layouts: 3.52 us -> none  [per_device(): rev_states = jnp.sum(reach[:, :, None, None] * all_backs, axis=0)[None]]
    dot_general x1, matrix products: 2.68 us -> 0.74 us  [per_device(): lax.dot_general(d_gate, gate_w, width_dims, preferred_element_type=jnp.fl...]
  transfers between devices with their start and end apart: 7 -> 0, of which waited for: 0 -> 0; matrix products, arithmetic and copies ran while one was open for 32% -> 0% of each run, Pallas kernels for 56% -> 0%
where the time goes in v2:
time: 141 us
  Pallas kernels  103 us (73%)
  matrix products  23.9 us (17%)
  local copies, waits for them, and re-layouts  8.04 us (6%)
  other arithmetic  4.56 us (3%)
    pallas_call x1, Pallas kernels, dispatch(): pl.pallas_call(functools.partial(dispatch_kernel, experts), out_shape=(fu...  41.6 us
    pallas_call x1, Pallas kernels, combine(): pl.pallas_call(functools.partial(combine_kernel, experts), out_shape=(jax...  37.7 us
    pallas_call x1, Pallas kernels, spread(): pl.pallas_call(functools.partial(spread_kernel, experts), out_shape=(jax....  24 us
    unnamed x29, local copies, waits for them, and re-layouts  5.75 us

profile of v2, /device:TPU:0, one launch (start us, length us, event | category | flops | bytes accessed | tf_op | source)
XLA Modules:
  0.0 140.7 jit_solution(3298104089192272719)
XLA Ops:
  0.7 0.9 copy.64
  4.0 2.1 %convolution_convert_fusion.3 = bf16[128,2048]{1,0:T(8,128)(2,1)} fusion(pred[128,128]{1,0:T(8,128)(4,1)S(1)} %compare_reduce_fusion, bf16[128,2048]{1,0:T(8,128)(2,1)} %param.13), kind=kOutput, calls=%fused_computation.9 | convolution fusion | flops 67371008 | bytes 1064960 | tf_op jit(solution)/shard_map/dot_general | solution.py:400
  6.1 0.8 fusion.37
  7.0 2.1 %fusion.3 = bf16[128,2048]{1,0:T(8,128)(2,1)} fusion(pred[128,128]{1,0:T(8,128)(4,1)S(1)} %compare_reduce_fusion, bf16[128,2048]{1,0:T(8,128)(2,1)} %own_cot.1, f32[128]{0:T(128)S(1)} %fusion.37), kind=kOutput, calls=%fused_computation.8 | convolution fusion | flops 67633152 | bytes 1065472 | tf_op jit(solution)/shard_map/dot_general | solution.py:401
  9.1 41.6 %shard_map.180 = (bf16[8,4,16,2048]{3,2,1,0:T(8,128)(2,1)}, bf16[8,4,16,2048]{3,2,1,0:T(8,128)(2,1)}) custom-call(bf16[8,16,2048]{2,1,0:T(8,128)(2,1)} %bitcast.135, bf16[8,16,2048]{2,1,0:T(8,128)(2,1)} %bitcast.136), custom_call_target="tpu_custom_call" | custom-call | tf_op jit(solution)/shard_map/pallas_call | solution.py:126
  50.8 2.5 %fusion.20 = f32[512,256]{1,0:T(8,128)S(1)} fusion(bf16[512,2048]{1,0:T(8,128)(2,1)} %bitcast.150, bf16[1,2048,256]{2,1,0:T(8,128)(2,1)S(1)} %copy-done.3), kind=kOutput, calls=%fused_computation.36 | convolution fusion | flops 536870912 | bytes 3670016 | tf_op jit(solution)/shard_map/dot_general | solution.py:445
  53.3 0.7 fusion.23
  54.1 0.9 copy-done.1
  55.2 0.8 multiply_convert_fusion.1
  56.0 1.7 %fusion = bf16[1,2048,256]{2,1,0:T(8,128)(2,1)} fusion(bf16[512,2048]{1,0:T(8,128)(2,1)S(1)} %bitcast.152, bf16[512,256]{1,0:T(8,128)(2,1)S(1)} %get-tuple-element.48), kind=kOutput, calls=%fused_computation.4 | convolution fusion | flops 537395200 | bytes 3407872 | tf_op jit(solution)/shard_map/dot_general | solution.py:348
  57.8 1.8 %fusion.1 = bf16[1,2048,256]{2,1,0:T(8,128)(2,1)} fusion(bf16[512,2048]{1,0:T(8,128)(2,1)S(1)} %bitcast.153, bf16[512,256]{1,0:T(8,128)(2,1)S(1)} %get-tuple-element.47), kind=kOutput, calls=%fused_computation.5 | convolution fusion | flops 537395200 | bytes 3407872 | tf_op jit(solution)/shard_map/dot_general | solution.py:351
  59.5 1.8 %fusion.2 = bf16[1,256,2048]{2,1,0:T(8,128)(2,1)} fusion(bf16[512,2048]{1,0:T(8,128)(2,1)S(1)} %bitcast.134, f32[512,256]{1,0:T(8,128)S(1)} %fusion.23, f32[512,256]{1,0:T(8,128)S(1)} %fusion.20), kind=kOutput, calls=%fused_computation.6 | convolution fusion | flops 538181632 | bytes 4194304 | tf_op jit(solution)/shard_map/dot_general | solution.py:354
  61.3 0.7 fusion.18
  62.0 2.1 %add_convert_fusion = bf16[512,2048]{1,0:T(8,128)(2,1)} fusion(f32[512,2048]{1,0:T(8,128)S(1)} %fusion.18, bf16[512,256]{1,0:T(8,128)(2,1)S(1)} %get-tuple-element.47, bf16[1,2048,256]{2,1,0:T(8,128)(2,1)S(1)} %copy-done.4), kind=kOutput, calls=%fused_computation | convolution fusion | flops 538968064 | bytes 7602176 | tf_op jit(solution)/shard_map/dot_general | solution.py:457
  64.9 37.7 %shard_map.181 = (bf16[128,2048]{1,0:T(8,128)(2,1)}, bf16[8,128,512]{2,1,0:T(8,128)(2,1)}) custom-call(bf16[8,64,2048]{2,1,0:T(8,128)(2,1)} %bitcast.132, bf16[128,512]{1,0:T(8,128)(2,1)} %convert_element_type.131.picks, bf16[128,2048]{1,0:T(8,128)(2,1)} %own_cot.1, bf16[128,512]{1,0:T(8,128)(2,1)} %out_rows.1), custom_call_target="tpu_custom_call" | custom-call | tf_op jit(solution)/shard_map/pallas_call | solution.py:243
  102.6 2.8 %fusion.50 = f32[128,512]{0,1:T(8,128)} fusion(bf16[128,2048]{1,0:T(8,128)(2,1)} %get-tuple-element.15.mixer, bf16[2048,512]{1,0:T(8,128)(2,1)S(1)} %copy-done), kind=kOutput, calls=%fused_computation.95 | convolution fusion | flops 268435456 | bytes 2883584 | tf_op jit(solution)/shard_map/dot_general | solution.py:489
  105.5 1.0 multiply_convert_fusion.4
  107.1 0.7 convert_element_type.137.state
  108.6 24.0 %shard_map.182 = (bf16[8,128,256]{2,1,0:T(8,128)(2,1)}, f32[256,128]{1,0:T(8,128)}) custom-call(bf16[128,2048]{1,0:T(8,128)(2,1)} %get-tuple-element.15.mixer, bf16[256,128]{1,0:T(8,128)(2,1)} %convert_element_type.137.state, f32[256,8]{1,0:T(8,128)} %bitcast.146), custom_call_target="tpu_custom_call" | custom-call | tf_op jit(solution)/shard_map/pallas_call | solution.py:310
  132.6 2.3 %convolution_bitcast_fusion = f32[256,512]{1,0:T(8,128)} fusion(bf16[8,128,256]{2,1,0:T(8,128)(2,1)} %get-tuple-element.16, bf16[8,128,512]{2,1,0:T(8,128)(2,1)S(1)} %copy-done.2), kind=kOutput, calls=%fused_computation.12 | convolution fusion | flops 268435456 | bytes 2097152 | tf_op jit(solution)/shard_map/dot_general | solution.py:541
  135.4 1.0 copy.71
  137.0 0.8 copy.73
  138.3 0.8 copy.74
  139.9 0.8 copy.75
  (61 shorter events, 7.3 us)
Async XLA Ops:
  0.6 102.0 %copy-start = (bf16[2048,512]{1,0:T(8,128)(2,1)S(1)}, bf16[2048,512]{1,0:T(8,128)(2,1)}, u32[]{:S(2)}) copy-start(bf16[2048,512]{1,0:T(8,128)(2,1)} %param.20) | copy-start | bytes 6291460
  0.6 50.1 %copy-start.3 = (bf16[1,2048,256]{2,1,0:T(8,128)(2,1)S(1)}, bf16[1,2048,256]{2,1,0:T(8,128)(2,1)}, u32[]{:S(2)}) copy-start(bf16[1,2048,256]{2,1,0:T(8,128)(2,1)} %param.17) | copy-start | bytes 3145732
  50.8 2.5 %copy-start.4 = (bf16[1,2048,256]{2,1,0:T(8,128)(2,1)S(1)}, bf16[1,2048,256]{2,1,0:T(8,128)(2,1)}, u32[]{:S(2)}) copy-start(bf16[1,2048,256]{2,1,0:T(8,128)(2,1)} %param.18) | copy-start | bytes 3145732
  50.8 2.5 %copy-start.9 = (bf16[8,4,16,2048]{3,2,1,0:T(8,128)(2,1)S(1)}, bf16[8,4,16,2048]{3,2,1,0:T(8,128)(2,1)}, u32[]{:S(2)}) copy-start(bf16[8,4,16,2048]{3,2,1,0:T(8,128)(2,1)} %get-tuple-element.13) | copy-start | bytes 6291460
  53.3 1.6 %copy-start.1 = (bf16[8,4,16,2048]{3,2,1,0:T(8,128)(2,1)S(1)}, bf16[8,4,16,2048]{3,2,1,0:T(8,128)(2,1)}, u32[]{:S(2)}) copy-start(bf16[8,4,16,2048]{3,2,1,0:T(8,128)(2,1)} %get-tuple-element.14) | copy-start | bytes 6291460
  53.3 1.9 %copy-start.10 = (bf16[1,256,2048]{2,1,0:T(8,128)(2,1)S(1)}, bf16[1,256,2048]{2,1,0:T(8,128)(2,1)}, u32[]{:S(2)}) copy-start(bf16[1,256,2048]{2,1,0:T(8,128)(2,1)} %param.19) | copy-start | bytes 3145732
  102.6 3.9 %copy-start.7 = (bf16[128,512]{1,0:T(8,128)(2,1)S(1)}, bf16[128,512]{1,0:T(8,128)(2,1)}, u32[]{:S(2)}) copy-start(bf16[128,512]{1,0:T(8,128)(2,1)} %param.21) | copy-start | bytes 393220
  102.6 30.0 %copy-start.2 = (bf16[8,128,512]{2,1,0:T(8,128)(2,1)S(1)}, bf16[8,128,512]{2,1,0:T(8,128)(2,1)}, u32[]{:S(2)}) copy-start(bf16[8,128,512]{2,1,0:T(8,128)(2,1)} %get-tuple-element.17) | copy-start | bytes 3145732
  107.8 27.0 %copy-start.8 = (bf16[128,512]{1,0:T(8,128)(2,1)S(1)}, bf16[128,512]{1,0:T(8,128)(2,1)}, u32[]{:S(2)}) copy-start(bf16[128,512]{1,0:T(8,128)(2,1)} %param.23) | copy-start | bytes 393220
  134.9 1.8 %copy-start.5 = (f32[1,8,64,64]{3,2,1,0:T(8,128)S(1)}, f32[1,8,64,64]{3,2,1,0:T(8,128)}, u32[]{:S(2)}) copy-start(f32[1,8,64,64]{3,2,1,0:T(8,128)} %param.25) | copy-start | bytes 393220
  134.9 2.9 %copy-start.6 = (f32[256,128]{1,0:T(8,128)S(1)}, f32[256,128]{1,0:T(8,128)}, u32[]{:S(2)}) copy-start(f32[256,128]{1,0:T(8,128)} %get-tuple-element.18) | copy-start | bytes 393220

commit v3 on v2

--- a/solution.py
+++ b/solution.py
@@ -72,21 +72,43 @@
 
 
 def dispatch_kernel(
-    experts, rows, cot, out_rows, out_cot, own, s_sp, r_sp, s_y, r_y, s_c, r_c
+    experts,
+    chosen,
+    weight,
+    rows_in,
+    cot_in,
+    out_rows,
+    out_cot,
+    rows,
+    cot,
+    own,
+    s_sp, r_sp, s_y, r_y, s_c, r_c
 ):
     me, tp, core, row, mate, across = seat(experts)
     greet(experts, me, (mate, across))
     arrays = ((rows, out_rows), (cot, out_cot))
+    share = out_rows.shape[2]
+
+    def block(src, index):
+        return src.at[pl.ds(pl.multiple_of(index * share, share), share)]
+
     far = {}
-    for k in range(1, experts):
-        peer = (me + k) % experts
-        for a, (src, dst) in enumerate(arrays):
+    for a, (src, dst) in enumerate(arrays):
+        if a == 0:
+            rows[...] = jnp.dot(
+                chosen[...], rows_in[...], preferred_element_type=jnp.float32
+            ).astype(jnp.bfloat16)
+        else:
+            picked = jnp.dot(chosen[...], cot_in[...], preferred_element_type=jnp.float32)
+            cot[...] = (weight[...] * picked).astype(jnp.bfloat16)
+        for k in range(1, experts):
+            peer = (me + k) % experts
             far[a, k] = send(
-                src.at[peer], dst.at[me, tp], s_sp.at[a, k], r_sp.at[a, k], {"sp": peer}
+                block(src, peer), dst.at[me, tp], s_sp.at[a, k], r_sp.at[a, k], {"sp": peer}
             )
     local = []
     for a, (src, dst) in enumerate(arrays):
-        copy = pltpu.make_async_copy(src.at[me], dst.at[me, tp], own.at[a])
+        copy = pltpu.make_async_copy(block(src, me), dst.at[me, tp], own.at[a])
         copy.start()
         local.append(copy)
     for copy in local:
@@ -119,16 +141,20 @@
             copy.wait_send()
 
 
-def dispatch(rows, cot, narrow):
-    experts, share, width = rows.shape
+def dispatch(chosen, weight, rows, cot, experts, narrow):
+    width = rows.shape[1]
+    share = chosen.shape[0] // experts
+    held = pltpu.VMEM((experts * share, width), jnp.bfloat16)
     full = jax.ShapeDtypeStruct((experts, narrow, share, width), rows.dtype)
     sem = pltpu.SemaphoreType.DMA
     return pl.pallas_call(
         functools.partial(dispatch_kernel, experts),
         out_shape=(full, full),
-        in_specs=[VMEM, VMEM],
+        in_specs=[VMEM] * 4,
         out_specs=(VMEM, VMEM),
         scratch_shapes=[
+            held,
+            held,
             sem((2,)),
             sem((2, experts)),
             sem((2, experts)),
@@ -138,7 +164,7 @@
             sem((2, 2, experts)),
         ],
         compiler_params=pltpu.CompilerParams(collective_id=0, has_side_effects=True),
-    )(rows, cot)
+    )(chosen, weight, rows, cot)
 
 
 def combine_kernel(
@@ -397,13 +423,8 @@
         hits = part_slot[:, None, None] == pair_slot[None]
         part_weight = jnp.sum(jnp.where(hits, route_weights[None], 0.0), axis=(1, 2))
         chosen = jnp.any(hits, axis=2).astype(jnp.bfloat16)
-        part_rows = jnp.dot(chosen, layer_input, preferred_element_type=jnp.float32)
-        part_cot = jnp.dot(chosen, out_cot, preferred_element_type=jnp.float32)
-        part_shape = (experts, share, model_width)
         got_rows, got_cot = dispatch(
-            part_rows.astype(jnp.bfloat16).reshape(part_shape),
-            (part_weight[:, None] * part_cot).astype(jnp.bfloat16).reshape(part_shape),
-            narrow,
+            chosen, part_weight[:, None], layer_input, out_cot, experts, narrow
         )
         all_slots = jnp.arange(experts * capacity, dtype=jnp.int32)
         picks = jnp.any(pair_slot[:, :, None] == all_slots[None, None], axis=1).astype(

time: 141 us -> 140 us (level); the launches traced: 141 us -> 138 us
  matrix products: 23.9 us -> 19.9 us
    dot_general x2 -> x0, matrix products: 4.27 us -> none  [the longest x1 2.14 us: per_device(): part_cot = jnp.dot(chosen, out_cot, preferred_element_type=jnp.float32)]
    pallas_call x1, Pallas kernels: 41.6 us -> 45.5 us  [dispatch(): pl.pallas_call(functools.partial(dispatch_kernel, experts), out_shape=(fu...]
    pallas_call x1, Pallas kernels: 37.7 us -> 34.7 us  [combine(): pl.pallas_call(functools.partial(combine_kernel, experts), out_shape=(jax...]
where the time goes in v3:
time: 140 us; the launch traced here: 138 us
  Pallas kernels  103 us (74%)
  matrix products  19.9 us (14%)
  local copies, waits for them, and re-layouts  8.85 us (6%)
  other arithmetic  5.19 us (4%)
    pallas_call x1, Pallas kernels, dispatch(): pl.pallas_call(functools.partial(dispatch_kernel, experts), out_shape=(fu...  45.5 us
    pallas_call x1, Pallas kernels, combine(): pl.pallas_call(functools.partial(combine_kernel, experts), out_shape=(jax...  34.7 us
    pallas_call x1, Pallas kernels, spread(): pl.pallas_call(functools.partial(spread_kernel, experts), out_shape=(jax....  23 us
    unnamed x29, local copies, waits for them, and re-layouts  5.8 us

profile of v3, /device:TPU:0, one launch (start us, length us, event | category | flops | bytes accessed | tf_op | source)
XLA Modules:
  0.0 138.0 jit_solution(6358180531177602554)
XLA Ops:
  0.6 0.9 copy.67
  3.0 0.7 multiply_add_fusion
  4.6 0.8 fusion.36
  5.5 0.8 copy.70.weight
  6.2 45.5 %shard_map.180 = (bf16[8,4,16,2048]{3,2,1,0:T(8,128)(2,1)}, bf16[8,4,16,2048]{3,2,1,0:T(8,128)(2,1)}) custom-call(bf16[128,128]{1,0:T(8,128)(2,1)} %convert_element_type.118.chosen, f32[128,1]{1,0:T(8,128)} %copy.70.weight, bf16[128,2048]{1,0:T(8,128)(2,1)} %rows_in.1, bf16[128,2048]{1,0:T(8,128)(2,1)} %own_cot.1), custom_call_target="tpu_custom_call" | custom-call | tf_op jit(solution)/shard_map/pallas_call | solution.py:150
  51.7 2.7 %fusion.19 = f32[512,256]{1,0:T(8,128)S(1)} fusion(bf16[512,2048]{1,0:T(8,128)(2,1)} %bitcast.144, bf16[1,2048,256]{2,1,0:T(8,128)(2,1)} %param.17), kind=kOutput, calls=%fused_computation.33 | convolution fusion | flops 536870912 | bytes 3670016 | tf_op jit(solution)/shard_map/dot_general | solution.py:466
  54.6 0.7 fusion.22
  55.3 0.9 copy-done.1
  56.4 0.8 multiply_convert_fusion.1
  57.3 1.7 %fusion = bf16[1,2048,256]{2,1,0:T(8,128)(2,1)} fusion(bf16[512,2048]{1,0:T(8,128)(2,1)S(1)} %bitcast.146, bf16[512,256]{1,0:T(8,128)(2,1)S(1)} %get-tuple-element.48), kind=kOutput, calls=%fused_computation.4 | convolution fusion | flops 537395200 | bytes 3407872 | tf_op jit(solution)/shard_map/dot_general | solution.py:374
  59.0 1.8 %fusion.1 = bf16[1,2048,256]{2,1,0:T(8,128)(2,1)} fusion(bf16[512,2048]{1,0:T(8,128)(2,1)S(1)} %bitcast.147, bf16[512,256]{1,0:T(8,128)(2,1)S(1)} %get-tuple-element.47), kind=kOutput, calls=%fused_computation.5 | convolution fusion | flops 537395200 | bytes 3407872 | tf_op jit(solution)/shard_map/dot_general | solution.py:377
  60.8 1.8 %fusion.2 = bf16[1,256,2048]{2,1,0:T(8,128)(2,1)} fusion(bf16[512,2048]{1,0:T(8,128)(2,1)S(1)} %bitcast.129, f32[512,256]{1,0:T(8,128)S(1)} %fusion.22, f32[512,256]{1,0:T(8,128)S(1)} %fusion.19), kind=kOutput, calls=%fused_computation.6 | convolution fusion | flops 538181632 | bytes 4194304 | tf_op jit(solution)/shard_map/dot_general | solution.py:380
  62.5 0.7 fusion.17
  63.3 2.1 %add_convert_fusion = bf16[512,2048]{1,0:T(8,128)(2,1)} fusion(f32[512,2048]{1,0:T(8,128)S(1)} %fusion.17, bf16[512,256]{1,0:T(8,128)(2,1)S(1)} %get-tuple-element.47, bf16[1,2048,256]{2,1,0:T(8,128)(2,1)S(1)} %copy-done.4), kind=kOutput, calls=%fused_computation | convolution fusion | flops 538968064 | bytes 7602176 | tf_op jit(solution)/shard_map/dot_general | solution.py:478
  66.2 34.7 %shard_map.181 = (bf16[128,2048]{1,0:T(8,128)(2,1)}, bf16[8,128,512]{2,1,0:T(8,128)(2,1)}) custom-call(bf16[8,64,2048]{2,1,0:T(8,128)(2,1)} %bitcast.127, bf16[128,512]{1,0:T(8,128)(2,1)} %convert_element_type.126.picks, bf16[128,2048]{1,0:T(8,128)(2,1)} %own_cot.1, bf16[128,512]{1,0:T(8,128)(2,1)} %out_rows.1), custom_call_target="tpu_custom_call" | custom-call | tf_op jit(solution)/shard_map/pallas_call | solution.py:269
  101.0 2.8 %fusion.49 = f32[128,512]{0,1:T(8,128)} fusion(bf16[128,2048]{1,0:T(8,128)(2,1)} %get-tuple-element.15.mixer, bf16[2048,512]{1,0:T(8,128)(2,1)S(1)} %copy-done), kind=kOutput, calls=%fused_computation.92 | convolution fusion | flops 268435456 | bytes 2883584 | tf_op jit(solution)/shard_map/dot_general | solution.py:510
  103.9 1.0 multiply_convert_fusion.4
  105.4 0.7 convert_element_type.132.state
  106.9 23.0 %shard_map.182 = (bf16[8,128,256]{2,1,0:T(8,128)(2,1)}, f32[256,128]{1,0:T(8,128)}) custom-call(bf16[128,2048]{1,0:T(8,128)(2,1)} %get-tuple-element.15.mixer, bf16[256,128]{1,0:T(8,128)(2,1)} %convert_element_type.132.state, f32[256,8]{1,0:T(8,128)} %bitcast.139), custom_call_target="tpu_custom_call" | custom-call | tf_op jit(solution)/shard_map/pallas_call | solution.py:336
  129.9 2.3 %convolution_bitcast_fusion = f32[256,512]{1,0:T(8,128)} fusion(bf16[8,128,256]{2,1,0:T(8,128)(2,1)} %get-tuple-element.16, bf16[8,128,512]{2,1,0:T(8,128)(2,1)S(1)} %copy-done.2), kind=kOutput, calls=%fused_computation.9 | convolution fusion | flops 268435456 | bytes 2097152 | tf_op jit(solution)/shard_map/dot_general | solution.py:562
  132.7 1.0 copy.75
  134.3 0.8 copy.77
  135.7 0.8 copy.78
  137.2 0.8 copy.79
  (61 shorter events, 7.3 us)
Async XLA Ops:
  0.6 100.3 %copy-start = (bf16[2048,512]{1,0:T(8,128)(2,1)S(1)}, bf16[2048,512]{1,0:T(8,128)(2,1)}, u32[]{:S(2)}) copy-start(bf16[2048,512]{1,0:T(8,128)(2,1)} %param.20) | copy-start | bytes 6291460
  51.7 2.7 %copy-start.4 = (bf16[1,2048,256]{2,1,0:T(8,128)(2,1)S(1)}, bf16[1,2048,256]{2,1,0:T(8,128)(2,1)}, u32[]{:S(2)}) copy-start(bf16[1,2048,256]{2,1,0:T(8,128)(2,1)} %param.18) | copy-start | bytes 3145732
  51.7 2.9 %copy-start.9 = (bf16[8,4,16,2048]{3,2,1,0:T(8,128)(2,1)S(1)}, bf16[8,4,16,2048]{3,2,1,0:T(8,128)(2,1)}, u32[]{:S(2)}) copy-start(bf16[8,4,16,2048]{3,2,1,0:T(8,128)(2,1)} %get-tuple-element.13) | copy-start | bytes 6291460
  54.6 1.6 %copy-start.1 = (bf16[8,4,16,2048]{3,2,1,0:T(8,128)(2,1)S(1)}, bf16[8,4,16,2048]{3,2,1,0:T(8,128)(2,1)}, u32[]{:S(2)}) copy-start(bf16[8,4,16,2048]{3,2,1,0:T(8,128)(2,1)} %get-tuple-element.14) | copy-start | bytes 6291460
  54.6 1.9 %copy-start.10 = (bf16[1,256,2048]{2,1,0:T(8,128)(2,1)S(1)}, bf16[1,256,2048]{2,1,0:T(8,128)(2,1)}, u32[]{:S(2)}) copy-start(bf16[1,256,2048]{2,1,0:T(8,128)(2,1)} %param.19) | copy-start | bytes 3145732
  60.8 1.8 %copy-start.3 = (bf16[1,2048,256]{2,1,0:T(8,128)(2,1)S(1)}, bf16[1,2048,256]{2,1,0:T(8,128)(2,1)}, u32[]{:S(2)}) copy-start(bf16[1,2048,256]{2,1,0:T(8,128)(2,1)} %param.17) | copy-start | bytes 3145732
  100.9 3.9 %copy-start.7 = (bf16[128,512]{1,0:T(8,128)(2,1)S(1)}, bf16[128,512]{1,0:T(8,128)(2,1)}, u32[]{:S(2)}) copy-start(bf16[128,512]{1,0:T(8,128)(2,1)} %param.21) | copy-start | bytes 393220
  100.9 29.0 %copy-start.2 = (bf16[8,128,512]{2,1,0:T(8,128)(2,1)S(1)}, bf16[8,128,512]{2,1,0:T(8,128)(2,1)}, u32[]{:S(2)}) copy-start(bf16[8,128,512]{2,1,0:T(8,128)(2,1)} %get-tuple-element.17) | copy-start | bytes 3145732
  106.2 26.0 %copy-start.8 = (bf16[128,512]{1,0:T(8,128)(2,1)S(1)}, bf16[128,512]{1,0:T(8,128)(2,1)}, u32[]{:S(2)}) copy-start(bf16[128,512]{1,0:T(8,128)(2,1)} %param.23) | copy-start | bytes 393220
  132.2 1.8 %copy-start.5 = (f32[1,8,64,64]{3,2,1,0:T(8,128)S(1)}, f32[1,8,64,64]{3,2,1,0:T(8,128)}, u32[]{:S(2)}) copy-start(f32[1,8,64,64]{3,2,1,0:T(8,128)} %param.25) | copy-start | bytes 393220
  132.2 2.9 %copy-start.6 = (f32[256,128]{1,0:T(8,128)S(1)}, f32[256,128]{1,0:T(8,128)}, u32[]{:S(2)}) copy-start(f32[256,128]{1,0:T(8,128)} %get-tuple-element.18) | copy-start | bytes 393220
